TPU v7x, 1024 devices: a whole 4x4x32 slice. The times are simulated.
1024 devices in a mesh: ep: 64 (over z, core), tp: 16 (over y, x).
Axes of the slice: x: 4, y: 4, z: 32, core: 2. Of those that a mesh axis runs over, the one named last changes fastest.
Arguments:
- tokens: bfloat16 [1024, 2048], P('ep'), may hold values from -6 to 6
- old_state: bfloat16 [1024, 256, 2048], P('ep', None, 'tp'), may hold values from -3 to 3
- first_gain: bfloat16 [2048], replicated, may hold values from 0.099609375 to 1.8984375
- query_weight: bfloat16 [2048, 1024], P('tp'), may hold values from -0.125 to 0.125
- key_weight: bfloat16 [2048, 1024], P('tp'), may hold values from -0.125 to 0.125
- value_weight: bfloat16 [2048, 2048], P(None, 'tp'), may hold values from -0.125 to 0.125
- outgate_weight: bfloat16 [2048, 2048], P(None, 'tp'), may hold values from -0.125 to 0.125
- lowrank_weight: bfloat16 [2048, 16], replicated, may hold values from -0.125 to 0.125
- decay_weight: bfloat16 [16, 1024], replicated, may hold values from -20 to 20
- decay_bias: float32 [1024], replicated, may hold values from -40 to 2
- head_gain: bfloat16 [2048], P('tp'), may hold values from 0.099609375 to 1.8984375
- output_weight: bfloat16 [2048, 2048], P('tp'), may hold values from -0.125 to 0.125
- second_gain: bfloat16 [2048], replicated, may hold values from 0.099609375 to 1.8984375
- expert_gate: bfloat16 [64, 2048, 1920], P('ep', None, 'tp'), may hold values from -0.125 to 0.125
- expert_up: bfloat16 [64, 2048, 1920], P('ep', None, 'tp'), may hold values from -0.125 to 0.125
- expert_down: bfloat16 [64, 1920, 2048], P('ep', 'tp'), may hold values from -0.125 to 0.125
- shared_gate: bfloat16 [2048, 1920], P(None, 'tp'), may hold values from -0.125 to 0.125
- shared_up: bfloat16 [2048, 1920], P(None, 'tp'), may hold values from -0.125 to 0.125
- shared_down: bfloat16 [1920, 2048], P('tp'), may hold values from -0.125 to 0.125
- route_ids: int32 [1024, 4], P('ep'), may hold values from 0 to 63, all different within a row; in each aligned block of 16 rows (0 to 15, 16 to 31, ...) at most 2 rows name the same one
- route_weights: float32 [1024, 4], P('ep'), may hold values from 0.1 to 1
Outputs:
- layer_out: bfloat16 [1024, 2048], P('ep', 'tp')
- new_state: bfloat16 [1024, 256, 2048], P('ep', None, 'tp')
Inputs may be any that keep to these rules, and one draw needn't show every extreme that they name: `route_ids`: within the rows of one device (aligned blocks of 16 rows) no expert is named more than 2 times, a bound that some block reaches.
All inputs are finite; a program needn't handle non-finite values.
Results may differ from a plain program's by a relative error of at most 0.035.
Values may be sent and summed in bfloat16 or wider, within the bound.
A program may use at most 32 MiB of HBM per device.

v0:
```python
import jax
import jax.numpy as jnp
from jax import lax
from jax.sharding import Mesh
from jax.sharding import PartitionSpec as P

TP = ("tp_0", "tp_1")
EP = ("ep_0", "ep_1")


EPSILON = 1e-06


def from_everyone(value, axis):
    devices = lax.axis_size(axis)
    return lax.all_to_all(
        jnp.broadcast_to(value[None], (devices, *value.shape)), axis, 0, 0, tiled=True
    )


def over_copies(value, axis):
    everything = from_everyone(value, axis)
    return jnp.sum(everything.astype(jnp.float32), axis=0)


def by_axis(value, axes):
    for axis in axes:
        value = lax.psum(value, axis)
    return value


def cut_along(value, dim, devices):
    before, after = (value.shape[:dim], value.shape[dim + 1 :])
    return jnp.moveaxis(value.reshape(*before, devices, -1, *after), dim, 0)


def sum_at_owner(value, axis, dim):
    devices = lax.axis_size(axis)
    pieces = lax.all_to_all(cut_along(value, dim, devices), axis, 0, 0, tiled=True)
    return jnp.sum(pieces.astype(jnp.float32), axis=0)


def joined_along(pieces, dim):
    pieces = jnp.moveaxis(pieces, 0, dim)
    lengths = pieces.shape
    return pieces.reshape(*lengths[:dim], lengths[dim] * lengths[dim + 1], *lengths[dim + 2 :])


def collect(value, axis, dim):
    return joined_along(from_everyone(value, axis), dim)


def moved_by_axis(pieces, axes, sequence):
    lengths = [lax.axis_size(a) for a in axes]
    pieces = pieces.reshape(*lengths, *pieces.shape[1:])
    for k in sequence:
        pieces = lax.all_to_all(pieces, axes[k], split_axis=k, concat_axis=k, tiled=True)
    return pieces.reshape(-1, *pieces.shape[len(axes) :])


def two_step_exchange(value, groups, sequence, split_dim, concat_dim):
    devices = lax.axis_size(groups[0]) * lax.axis_size(groups[1])
    pieces = cut_along(value, split_dim, devices)
    return joined_along(moved_by_axis(pieces, groups, sequence), concat_dim)


def rms_norm(values, norm_gain):
    floats = values.astype(jnp.float32)
    scaled = floats * lax.rsqrt(jnp.mean(floats * floats, axis=-1, keepdims=True) + EPSILON)
    return (scaled * norm_gain.astype(jnp.float32)).astype(jnp.bfloat16)


def project(left_side, right_side):
    return jnp.dot(left_side, right_side, preferred_element_type=jnp.float32)


def body(
    tokens,
    old_state,
    first_gain,
    query_weight,
    key_weight,
    value_weight,
    outgate_weight,
    lowrank_weight,
    decay_weight,
    decay_bias,
    head_gain,
    output_weight,
    second_gain,
    expert_gate,
    expert_up,
    expert_down,
    shared_gate,
    shared_up,
    shared_down,
    route_ids,
    route_weights,
):
    tp_count = lax.axis_size(TP)
    ep_count = lax.axis_size(EP)
    tp_index = lax.axis_index(TP)
    seq_count, model_width = tokens.shape
    key_width = old_state.shape[1]
    value_count = old_state.shape[2]
    head_count = decay_weight.shape[1] // key_width
    head_width = value_count * tp_count // head_count
    head_index = tp_index * value_count // head_width
    feature_cols = model_width // tp_count
    normed = rms_norm(tokens, first_gain)
    own_normed = lax.dynamic_slice_in_dim(normed, tp_index * feature_cols, feature_cols, 1)
    query_sum, key_sum = (
        over_copies(project(own_normed, query_weight).astype(jnp.bfloat16), TP).astype(jnp.float32),
        over_copies(project(own_normed, key_weight).astype(jnp.bfloat16), TP).astype(jnp.float32),
    )
    offset = head_index * key_width
    query_rows = lax.dynamic_slice_in_dim(query_sum.astype(jnp.bfloat16), offset, key_width, 1)
    key_rows = lax.dynamic_slice_in_dim(key_sum.astype(jnp.bfloat16), offset, key_width, 1)
    value_rows = project(normed, value_weight).astype(jnp.bfloat16)
    out_gate = project(normed, outgate_weight).astype(jnp.bfloat16)
    lowrank = project(normed, lowrank_weight).astype(jnp.bfloat16)
    decay_cols = lax.dynamic_slice_in_dim(decay_weight, offset, key_width, 1)
    bias_cols = lax.dynamic_slice_in_dim(decay_bias, offset, key_width, 0)
    log_decay = jax.nn.log_sigmoid(project(lowrank, decay_cols) + bias_cols) / 16.0
    carried = (
        jnp.exp(log_decay)[:, :, None] * old_state.astype(jnp.float32)
        + key_rows.astype(jnp.float32)[:, :, None] * value_rows.astype(jnp.float32)[:, None, :]
    )
    new_state = carried.astype(jnp.bfloat16)
    read_out = jnp.einsum(
        "bi,bic->bc", query_rows.astype(jnp.float32), carried, precision=lax.Precision.HIGHEST
    ) * key_width ** (-0.5)
    own_squares = jnp.sum(read_out * read_out, axis=1)
    mixed_rows = (
        read_out * head_gain.astype(jnp.float32) * jax.nn.silu(out_gate.astype(jnp.float32))
    ).astype(jnp.bfloat16)
    partial_value = project(mixed_rows, output_weight)
    selector = (jnp.arange(head_count) == head_index).astype(jnp.float32)
    head_squares = own_squares[:, None] * selector[None, :]
    square_sums = by_axis(head_squares, TP)
    inverse = lax.rsqrt(square_sums / head_width + EPSILON)
    own_inverse = jnp.sum(inverse * selector[None, :], axis=1)
    attended = over_copies((partial_value * own_inverse[:, None]).astype(jnp.bfloat16), TP).astype(
        jnp.float32
    )
    second = (tokens.astype(jnp.float32) + attended).astype(jnp.bfloat16)
    normed_two = rms_norm(second, second_gain)
    shared_hidden = (
        jax.nn.silu(project(normed_two, shared_gate)) * project(normed_two, shared_up)
    ).astype(jnp.bfloat16)
    shared_own = sum_at_owner(project(shared_hidden, shared_down).astype(jnp.bfloat16), TP, 1)
    local_experts = expert_gate.shape[0]
    expert_count = local_experts * ep_count
    top_count = route_ids.shape[1]
    capacity = max(2, (2 * seq_count * top_count + expert_count - 1) // expert_count)
    flat_ids = route_ids.reshape(-1)
    onehot = (flat_ids[:, None] == jnp.arange(expert_count, dtype=jnp.int32)[None, :]).astype(
        jnp.int32
    )
    slot_rank = jnp.sum((jnp.cumsum(onehot, axis=0) - onehot) * onehot, axis=1)
    target = flat_ids * capacity + slot_rank
    placing = (
        target[None, :] == jnp.arange(expert_count * capacity, dtype=jnp.int32)[:, None]
    ).astype(jnp.bfloat16)
    sources = lax.dynamic_slice_in_dim(normed_two, tp_index * feature_cols, feature_cols, 1)
    dispatched = project(placing, jnp.repeat(sources, top_count, axis=0)).astype(jnp.bfloat16)
    dispatched = dispatched.reshape(expert_count, capacity, sources.shape[1])
    received = lax.all_to_all(dispatched, EP, split_axis=0, concat_axis=0, tiled=True)
    received = collect(received, TP, 2)
    slot_count = received.shape[1]
    grouped = received.reshape(ep_count, local_experts, slot_count, model_width)
    grouped = grouped.transpose(1, 0, 2, 3).reshape(
        local_experts, ep_count * slot_count, model_width
    )
    gate_vals = jnp.einsum("erd,edf->erf", grouped, expert_gate, preferred_element_type=jnp.float32)
    up_vals = jnp.einsum("erd,edf->erf", grouped, expert_up, preferred_element_type=jnp.float32)
    hidden = (jax.nn.silu(gate_vals) * up_vals).astype(jnp.bfloat16)
    down_vals = jnp.einsum("erf,efd->erd", hidden, expert_down, preferred_element_type=jnp.float32)
    summed = sum_at_owner(down_vals.astype(jnp.bfloat16), TP, 2).astype(jnp.bfloat16)
    regrouped = summed.reshape(local_experts, ep_count, slot_count, feature_cols)
    regrouped = regrouped.transpose(1, 0, 2, 3).reshape(expert_count, slot_count, feature_cols)
    returned = two_step_exchange(regrouped, ("ep_0", "ep_1"), (1, 0), 0, 0)
    picked = returned.reshape(expert_count * capacity, feature_cols)[target]
    picked = picked.astype(jnp.float32).reshape(seq_count, top_count, feature_cols)
    routed = jnp.sum(picked * route_weights[:, :, None], axis=1)
    own_second = lax.dynamic_slice_in_dim(second, tp_index * feature_cols, feature_cols, 1).astype(
        jnp.float32
    )
    layer_out = (own_second + shared_own + routed).astype(jnp.bfloat16)
    return (layer_out, new_state)


def solution(mesh):
    torus = Mesh(mesh.devices.reshape(32, 2, 4, 4), ("ep_0", "ep_1", "tp_0", "tp_1"))
    return jax.shard_map(
        body,
        mesh=torus,
        in_specs=(
            P(EP, None),
            P(EP, None, TP),
            P(),
            P(TP, None),
            P(TP, None),
            P(None, TP),
            P(None, TP),
            P(),
            P(),
            P(),
            P(TP),
            P(TP, None),
            P(),
            P(EP, None, TP),
            P(EP, None, TP),
            P(EP, TP, None),
            P(None, TP),
            P(None, TP),
            P(TP, None),
            P(EP, None),
            P(EP, None),
        ),
        out_specs=(P(EP, TP), P(EP, None, TP)),
        check_vma=False,
    )
```

profile of v0, /device:TPU:1, one launch (start us, length us, event | category | flops | bytes accessed | tf_op | source)
XLA Modules:
  0.0 205.7 jit_solution(3653478440204996607)
XLA Ops:
  0.6 0.0 copy-start
  0.7 0.7 convert_element_type.116
  1.4 1.0 fusion.27
  2.4 1.0 fusion.29
  3.4 1.1 convolution_convert_fusion.4
  4.5 0.9 broadcast_in_dim.10
  5.4 7.6 %all-to-all-start = ((bf16[16,16,1024]{2,1,0:T(8,128)(2,1)}), bf16[16,16,1024]{2,1,0:T(8,128)(2,1)S(1)}, u32[]{:S(2)}, u32[]{:S(2)}) async-start(bf16[16,16,1024]{2,1,0:T(8,128)(2,1)} %broadcast_in_dim.10), calls=%async_computation | async-start | bytes 1048576 | tf_op jit(solution)/shard_map/all_to_all | solution.py:16
  13.0 0.8 dynamic_slice.24
  13.8 1.0 fusion.42
  14.8 0.1 convolution_convert_fusion.3
  15.0 7.0 %all-to-all-done = bf16[16,16,1024]{2,1,0:T(8,128)(2,1)S(1)} async-done(((bf16[16,16,1024]{2,1,0:T(8,128)(2,1)}), bf16[16,16,1024]{2,1,0:T(8,128)(2,1)S(1)}, u32[]{:S(2)}, u32[]{:S(2)}) %all-to-all-start) | async-done | bytes 524320 | tf_op jit(solution)/shard_map/all_to_all | solution.py:16
  21.9 0.9 broadcast_in_dim.11
  22.8 3.6 %all-to-all-start.1 = ((bf16[16,16,1024]{2,1,0:T(8,128)(2,1)}), bf16[16,16,1024]{2,1,0:T(8,128)(2,1)S(1)}, u32[]{:S(2)}, u32[]{:S(2)}) async-start(bf16[16,16,1024]{2,1,0:T(8,128)(2,1)} %broadcast_in_dim.11), calls=%async_computation.1 | async-start | bytes 1048576 | tf_op jit(solution)/shard_map/all_to_all | solution.py:16
  26.4 0.2 fusion.9
  26.6 0.1 reduce_sum.111
  26.7 8.6 %all-to-all-done.1 = bf16[16,16,1024]{2,1,0:T(8,128)(2,1)S(1)} async-done(((bf16[16,16,1024]{2,1,0:T(8,128)(2,1)}), bf16[16,16,1024]{2,1,0:T(8,128)(2,1)S(1)}, u32[]{:S(2)}, u32[]{:S(2)}) %all-to-all-start.1) | async-done | bytes 524320 | tf_op jit(solution)/shard_map/all_to_all | solution.py:16
  35.3 0.1 reduce_sum.112
  35.4 1.8 fusion.2
  37.2 0.1 multiply_reduce_fusion
  37.3 0.1 broadcast_multiply_fusion.1
  37.3 6.8 %psum.14 = f32[16,4]{0,1:T(4,128)S(1)} all-reduce(f32[16,4]{0,1:T(4,128)S(1)} %broadcast_multiply_fusion.1), channel_id=1, replica_groups=mesh['ep_0'=32,'ep_1'=2,'tp_0'=4,'tp_1'=4] {'tp_0'}, use_global_device_ids=true, to_apply=%region_4.5 | all-reduce | flops 64 | bytes 512 | tf_op jit(solution)/shard_map/psum | solution.py:28
  44.2 6.9 %psum.15 = f32[16,4]{0,1:T(4,128)S(1)} all-reduce(f32[16,4]{0,1:T(4,128)S(1)} %psum.14), channel_id=1, replica_groups=mesh['ep_0'=32,'ep_1'=2,'tp_0'=4,'tp_1'=4] {'tp_1'}, use_global_device_ids=true, to_apply=%region_5.6 | all-reduce | flops 64 | bytes 512 | tf_op jit(solution)/shard_map/psum | solution.py:28
  51.0 0.1 multiply_reduce_fusion.1
  51.1 0.4 fusion
  51.5 1.1 broadcast_in_dim.12
  52.6 3.8 %all-to-all-start.2 = ((bf16[16,16,2048]{2,1,0:T(8,128)(2,1)}), bf16[16,16,2048]{2,1,0:T(8,128)(2,1)S(1)}, u32[]{:S(2)}, u32[]{:S(2)}) async-start(bf16[16,16,2048]{2,1,0:T(8,128)(2,1)} %broadcast_in_dim.12), calls=%async_computation.2 | async-start | bytes 2097152 | tf_op jit(solution)/shard_map/all_to_all | solution.py:16
  56.4 0.1 copy.45
  56.5 0.1 reshape.127
  56.6 0.1 fusion.38
  56.7 0.1 reduce_window_sum.11
  56.8 0.2 select_reduce_fusion
  57.0 11.6 %all-to-all-done.2 = bf16[16,16,2048]{2,1,0:T(8,128)(2,1)S(1)} async-done(((bf16[16,16,2048]{2,1,0:T(8,128)(2,1)}), bf16[16,16,2048]{2,1,0:T(8,128)(2,1)S(1)}, u32[]{:S(2)}, u32[]{:S(2)}) %all-to-all-start.2) | async-done | bytes 1048608 | tf_op jit(solution)/shard_map/all_to_all | solution.py:16
  68.6 0.1 convert_reduce_fusion
  68.8 0.1 fusion.24
  68.9 0.1 fusion.26
  69.0 0.1 convolution_convert_fusion.2
  69.2 60.7 %all_to_all.45 = bf16[64,2,128]{2,1,0:T(2,128)(2,1)S(1)} all-to-all(bf16[64,2,128]{2,1,0:T(2,128)(2,1)S(1)} %bitcast.71), channel_id=1, replica_groups=mesh['ep_0'=32,'ep_1'=2,'tp_0'=4,'tp_1'=4] {'ep_0','ep_1'}, dimensions={0} | all-to-all | bytes 65536 | tf_op jit(solution)/shard_map/all_to_all | solution.py:168
  129.9 1.2 broadcast_in_dim.14
  131.1 3.7 %all-to-all-start.5 = ((bf16[16,64,2,128]{3,2,1,0:T(2,128)(2,1)}), bf16[16,64,2,128]{3,2,1,0:T(2,128)(2,1)S(1)}, u32[]{:S(2)}, u32[]{:S(2)}) async-start(bf16[16,64,2,128]{3,2,1,0:T(2,128)(2,1)} %broadcast_in_dim.14), calls=%async_computation.5 | async-start | bytes 1048576 | tf_op jit(solution)/shard_map/all_to_all | solution.py:16
  134.8 0.1 copy.50
  134.9 0.1 mul.219
  135.0 9.9 %all-to-all-done.5 = bf16[16,64,2,128]{3,2,1,0:T(2,128)(2,1)S(1)} async-done(((bf16[16,64,2,128]{3,2,1,0:T(2,128)(2,1)}), bf16[16,64,2,128]{3,2,1,0:T(2,128)(2,1)S(1)}, u32[]{:S(2)}, u32[]{:S(2)}) %all-to-all-start.5) | async-done | bytes 524320 | tf_op jit(solution)/shard_map/all_to_all | solution.py:16
  144.9 0.6 copy.46
  145.5 0.3 fusion.15
  145.8 2.0 fusion.3
  147.8 0.1 copy.56
  148.0 0.9 copy.70
  148.9 3.7 %all-to-all-start.6 = ((bf16[16,1,128,128]{3,2,1,0:T(8,128)(2,1)}), bf16[16,1,128,128]{3,2,1,0:T(8,128)(2,1)S(1)}, u32[]{:S(2)}, u32[]{:S(2)}) async-start(bf16[16,1,128,128]{3,2,1,0:T(8,128)(2,1)} %bitcast.62), calls=%async_computation.6 | async-start | bytes 1048576 | tf_op jit(solution)/shard_map/all_to_all | solution.py:39
  152.6 0.1 copy.51
  152.7 0.2 fusion.64
  153.0 1.6 fusion.4
  154.5 0.7 copy.71
  155.2 6.7 %all-to-all-done.6 = bf16[16,1,128,128]{3,2,1,0:T(8,128)(2,1)S(1)} async-done(((bf16[16,1,128,128]{3,2,1,0:T(8,128)(2,1)}), bf16[16,1,128,128]{3,2,1,0:T(8,128)(2,1)S(1)}, u32[]{:S(2)}, u32[]{:S(2)}) %all-to-all-start.6) | async-done | bytes 524320 | tf_op jit(solution)/shard_map/all_to_all | solution.py:39
  161.9 0.1 reduce_sum.119
  162.0 6.6 %all_to_all.46 = bf16[32,2,1,2,128]{4,3,0,2,1:T(2,128)(2,1)S(1)} all-to-all(bf16[32,2,1,2,128]{4,3,0,2,1:T(2,128)(2,1)S(1)} %copy.48), channel_id=1, replica_groups=mesh['ep_0'=32,'ep_1'=2,'tp_0'=4,'tp_1'=4] {'ep_1'}, dimensions={1} | all-to-all | bytes 65536 | tf_op jit(solution)/shard_map/all_to_all | solution.py:57
  168.6 3.5 %all-to-all-start.3 = ((bf16[16,16,128]{2,1,0:T(8,128)(2,1)}), bf16[16,16,128]{2,1,0:T(8,128)(2,1)S(1)}, u32[]{:S(2)}, u32[]{:S(2)}) async-start(bf16[16,16,128]{2,1,0:T(8,128)(2,1)} %bitcast.64), calls=%async_computation.3 | async-start | bytes 131072 | tf_op jit(solution)/shard_map/all_to_all | solution.py:39
  172.1 0.6 copy.49
  172.7 5.8 %all-to-all-done.3 = bf16[16,16,128]{2,1,0:T(8,128)(2,1)S(1)} async-done(((bf16[16,16,128]{2,1,0:T(8,128)(2,1)}), bf16[16,16,128]{2,1,0:T(8,128)(2,1)S(1)}, u32[]{:S(2)}, u32[]{:S(2)}) %all-to-all-start.3) | async-done | bytes 65568 | tf_op jit(solution)/shard_map/all_to_all | solution.py:39
  178.5 3.8 %all-to-all-start.8 = ((bf16[32,2,1,2,128]{4,3,1,2,0:T(2,128)(2,1)}), bf16[32,2,1,2,128]{4,3,1,2,0:T(2,128)(2,1)S(1)}, u32[]{:S(2)}, u32[]{:S(2)}) async-start(bf16[32,2,1,2,128]{4,3,1,2,0:T(2,128)(2,1)} %copy.49), calls=%async_computation.8 | async-start | bytes 65536 | tf_op jit(solution)/shard_map/all_to_all | solution.py:57
  182.4 2.0 fusion.1
  184.4 19.9 %all-to-all-done.8 = bf16[32,2,1,2,128]{4,3,1,2,0:T(2,128)(2,1)S(1)} async-done(((bf16[32,2,1,2,128]{4,3,1,2,0:T(2,128)(2,1)}), bf16[32,2,1,2,128]{4,3,1,2,0:T(2,128)(2,1)S(1)}, u32[]{:S(2)}, u32[]{:S(2)}) %all-to-all-start.8) | async-done | bytes 32800 | tf_op jit(solution)/shard_map/all_to_all | solution.py:57
  204.4 0.6 gather_fusion
  205.0 0.1 fusion.36
  205.1 0.6 add_convert_fusion
  (42 shorter events, 0.2 us)
Async XLA Ops:
  0.6 50.5 %copy-start = (bf16[128,2048]{1,0:T(8,128)(2,1)S(1)}, bf16[128,2048]{1,0:T(8,128)(2,1)}, u32[]{:S(2)}) copy-start(bf16[128,2048]{1,0:T(8,128)(2,1)} %param.32) | copy-start | bytes 1572868
  2.4 11.4 %copy-start.12 = (bf16[2048,16]{0,1:T(8,128)(2,1)S(1)}, bf16[2048,16]{0,1:T(8,128)(2,1)}, u32[]{:S(2)}) copy-start(bf16[2048,16]{0,1:T(8,128)(2,1)} %param.28) | copy-start | bytes 196612
  3.3 11.5 %copy-start.8 = (bf16[128,1024]{1,0:T(8,128)(2,1)S(1)}, bf16[128,1024]{1,0:T(8,128)(2,1)}, u32[]{:S(2)}) copy-start(bf16[128,1024]{1,0:T(8,128)(2,1)} %param.25) | copy-start | bytes 786436
  5.4 16.6 %all-to-all-start = ((bf16[16,16,1024]{2,1,0:T(8,128)(2,1)}), bf16[16,16,1024]{2,1,0:T(8,128)(2,1)S(1)}, u32[]{:S(2)}, u32[]{:S(2)}) async-start(bf16[16,16,1024]{2,1,0:T(8,128)(2,1)} %broadcast_in_dim.10), calls=%async_computation | async-start | bytes 1048576 | tf_op jit(solution)/shard_map/all_to_all | solution.py:16
  12.9 13.4 %copy-start.13 = (bf16[128]{0:T(256)(128)(2,1)S(1)}, bf16[128]{0:T(256)(128)(2,1)}, u32[]{:S(2)}) copy-start(bf16[128]{0:T(256)(128)(2,1)} %param.31) | copy-start | bytes 772
  13.0 13.4 %copy-start.3 = (bf16[2048,128]{1,0:T(8,128)(2,1)S(1)}, bf16[2048,128]{1,0:T(8,128)(2,1)}, u32[]{:S(2)}) copy-start(bf16[2048,128]{1,0:T(8,128)(2,1)} %param.26) | copy-start | bytes 1572868
  22.8 12.5 %all-to-all-start.1 = ((bf16[16,16,1024]{2,1,0:T(8,128)(2,1)}), bf16[16,16,1024]{2,1,0:T(8,128)(2,1)S(1)}, u32[]{:S(2)}, u32[]{:S(2)}) async-start(bf16[16,16,1024]{2,1,0:T(8,128)(2,1)} %broadcast_in_dim.11), calls=%async_computation.1 | async-start | bytes 1048576 | tf_op jit(solution)/shard_map/all_to_all | solution.py:16
  26.4 9.0 %copy-start.1 = (bf16[16,256,128]{2,1,0:T(8,128)(2,1)S(1)}, bf16[16,256,128]{2,1,0:T(8,128)(2,1)}, u32[]{:S(2)}) copy-start(bf16[16,256,128]{2,1,0:T(8,128)(2,1)} %param.22) | copy-start | bytes 3145732
  35.4 15.7 %copy-start.4 = (bf16[2048,128]{1,0:T(8,128)(2,1)S(1)}, bf16[2048,128]{1,0:T(8,128)(2,1)}, u32[]{:S(2)}) copy-start(bf16[2048,128]{1,0:T(8,128)(2,1)} %param.27) | copy-start | bytes 1572868
  52.6 3.8 %copy-start.10 = (bf16[2048]{0:T(1024)(128)(2,1)S(1)}, bf16[2048]{0:T(1024)(128)(2,1)}, u32[]{:S(2)}) copy-start(bf16[2048]{0:T(1024)(128)(2,1)} %param.33) | copy-start | bytes 12292
  52.6 3.8 %copy-start.9 = (s32[16,4]{0,1:T(4,128)S(1)}, s32[16,4]{0,1:T(4,128)}, u32[]{:S(2)}) copy-start(s32[16,4]{0,1:T(4,128)} %param.40) | copy-start | bytes 772
  52.6 16.0 %all-to-all-start.2 = ((bf16[16,16,2048]{2,1,0:T(8,128)(2,1)}), bf16[16,16,2048]{2,1,0:T(8,128)(2,1)S(1)}, u32[]{:S(2)}, u32[]{:S(2)}) async-start(bf16[16,16,2048]{2,1,0:T(8,128)(2,1)} %broadcast_in_dim.12), calls=%async_computation.2 | async-start | bytes 2097152 | tf_op jit(solution)/shard_map/all_to_all | solution.py:16
  56.4 12.3 %copy-start.2 = (bf16[16,2048]{1,0:T(8,128)(2,1)S(1)}, bf16[16,2048]{1,0:T(8,128)(2,1)}, u32[]{:S(2)}) copy-start(bf16[16,2048]{1,0:T(8,128)(2,1)} %param.21) | copy-start | bytes 196612
  131.1 14.4 %copy-start.5 = (bf16[1,2048,120]{1,2,0:T(8,128)(2,1)S(1)}, bf16[1,2048,120]{1,2,0:T(8,128)(2,1)}, u32[]{:S(2)}) copy-start(bf16[1,2048,120]{1,2,0:T(8,128)(2,1)} %param.34) | copy-start | bytes 1474564
  131.1 13.8 %all-to-all-start.5 = ((bf16[16,64,2,128]{3,2,1,0:T(2,128)(2,1)}), bf16[16,64,2,128]{3,2,1,0:T(2,128)(2,1)S(1)}, u32[]{:S(2)}, u32[]{:S(2)}) async-start(bf16[16,64,2,128]{3,2,1,0:T(2,128)(2,1)} %broadcast_in_dim.14), calls=%async_computation.5 | async-start | bytes 1048576 | tf_op jit(solution)/shard_map/all_to_all | solution.py:16
  148.0 4.7 %copy-start.11 = (f32[16,4]{0,1:T(4,128)S(1)}, f32[16,4]{0,1:T(4,128)}, u32[]{:S(2)}) copy-start(f32[16,4]{0,1:T(4,128)} %param.41) | copy-start | bytes 772
  148.0 4.8 %copy-start.6 = (bf16[2048,120]{0,1:T(8,128)(2,1)S(1)}, bf16[2048,120]{0,1:T(8,128)(2,1)}, u32[]{:S(2)}) copy-start(bf16[2048,120]{0,1:T(8,128)(2,1)} %param.37) | copy-start | bytes 1474564
  148.9 4.1 %copy-start.7 = (bf16[120,2048]{1,0:T(8,128)(2,1)S(1)}, bf16[120,2048]{1,0:T(8,128)(2,1)}, u32[]{:S(2)}) copy-start(bf16[120,2048]{1,0:T(8,128)(2,1)} %param.39) | copy-start | bytes 1474564
  148.9 13.0 %all-to-all-start.6 = ((bf16[16,1,128,128]{3,2,1,0:T(8,128)(2,1)}), bf16[16,1,128,128]{3,2,1,0:T(8,128)(2,1)S(1)}, u32[]{:S(2)}, u32[]{:S(2)}) async-start(bf16[16,1,128,128]{3,2,1,0:T(8,128)(2,1)} %bitcast.62), calls=%async_computation.6 | async-start | bytes 1048576 | tf_op jit(solution)/shard_map/all_to_all | solution.py:39
  168.6 10.0 %all-to-all-start.3 = ((bf16[16,16,128]{2,1,0:T(8,128)(2,1)}), bf16[16,16,128]{2,1,0:T(8,128)(2,1)S(1)}, u32[]{:S(2)}, u32[]{:S(2)}) async-start(bf16[16,16,128]{2,1,0:T(8,128)(2,1)} %bitcast.64), calls=%async_computation.3 | async-start | bytes 131072 | tf_op jit(solution)/shard_map/all_to_all | solution.py:39
  178.5 25.8 %all-to-all-start.8 = ((bf16[32,2,1,2,128]{4,3,1,2,0:T(2,128)(2,1)}), bf16[32,2,1,2,128]{4,3,1,2,0:T(2,128)(2,1)S(1)}, u32[]{:S(2)}, u32[]{:S(2)}) async-start(bf16[32,2,1,2,128]{4,3,1,2,0:T(2,128)(2,1)} %copy.49), calls=%async_computation.8 | async-start | bytes 65536 | tf_op jit(solution)/shard_map/all_to_all | solution.py:57
where the time goes:
time: 207 us; the launch traced here: 206 us
  blocking collectives  81 us (39%)
  waiting for transfers between devices  69.5 us (34%)
  starting transfers between devices  29.7 us (14%)
  local copies, waits for them, and re-layouts  8.95 us (4%)
  matrix products  8.84 us (4%)
  other arithmetic  6.72 us (3%)
    all_to_all x1, blocking collectives, body(): lax.all_to_all(dispatched, EP, split_axis=0, concat_axis=0, tiled=True)  60.7 us
    all_to_all x4, waiting for transfers between devices, from_everyone(): lax.all_to_all(jnp.broadcast_to(value[None], (devices, *value.shape)), ax...  37 us
    all_to_all x1, waiting for transfers between devices, moved_by_axis(): lax.all_to_all(pieces, axes[k], split_axis=k, concat_axis=k, tiled=True)  19.9 us
    all_to_all x4, starting transfers between devices, from_everyone(): lax.all_to_all(jnp.broadcast_to(value[None], (devices, *value.shape)), ax...  18.6 us
    psum x2, blocking collectives, by_axis(): value = lax.psum(value, axis)  13.7 us
    all_to_all x2, waiting for transfers between devices, sum_at_owner(): lax.all_to_all(cut_along(value, dim, devices), axis, 0, 0, tiled=True)  12.5 us
    all_to_all x2, starting transfers between devices, sum_at_owner(): lax.all_to_all(cut_along(value, dim, devices), axis, 0, 0, tiled=True)  7.2 us
    all_to_all x1, blocking collectives, moved_by_axis(): lax.all_to_all(pieces, axes[k], split_axis=k, concat_axis=k, tiled=True)  6.57 us
  transfers between devices with their start and end apart: 7, of which 7 were waited for; matrix products, arithmetic and copies ran while one was open for 4% of the time, Pallas kernels for 0%

commit v1 on v0

v1 whole, which is shorter than its diff:
```python
import functools

import jax
import jax.numpy as jnp
from jax import lax
from jax.experimental import pallas as pl
from jax.experimental.pallas import tpu as pltpu
from jax.sharding import PartitionSpec as P

EPSILON = 1e-06
LANES = 128
CHUNKS = 4
MESH = pl.DeviceIdType.MESH
F32 = jnp.float32
BF16 = jnp.bfloat16


def dot(left, right):
    return jnp.dot(left, right, preferred_element_type=F32)


def dot_t(left, right):
    return lax.dot_general(left, right, (((1,), (1,)), ((), ())), preferred_element_type=F32)


def silu(x):
    return x / (1.0 + jnp.exp(-x))


def kernel(
    sizes,
    tokens_h, state_h, gain1_h, wq_h, wk_h, wv_h, wo_h, wl_h, wd_h, bias_h, hgain_h, wout_h, gain2_h,
    eg_h, eu_h, ed_h, sg_h, su_h, sd_h, ids_h, rw_h,
    out_h, newstate_h,
    tokens, state, gain1, wq, wk, wv, wo, wl, wd, bias, hgain, wout, gain2, eg, eu, ed, sg, su, sd, ids, rw,
    normed, own_normed, a_send, a_recv, b_send, b_recv, c_send, c_recv, n2, s_send, s_recv,
    d_send, d_recv, e_send, e_recv, xn, g_send, g_recv, h_send, h_recv, newstate, out,
    in_sem, out_sem, a_sem, b_sem, c_sem, s_sem, d_sem, e_sem, g_sem, h_sem,
):
    n_ep, n_tp, heads, chunks = sizes
    seqs, width = tokens.shape
    dk, vc = state.shape[1], state.shape[2]
    blocks = width // LANES
    per_head = n_tp // heads
    head_width = vc * per_head
    slots = n_ep * 2
    n_chunk = n_ep // chunks
    rows = n_chunk * 2
    p = lax.axis_index("ep")
    t = lax.axis_index("tp")
    head = t // per_head
    own_cols = pl.ds(pl.multiple_of(t * LANES, LANES), LANES)

    def tp_peer(k):
        return lax.rem(t + k, n_tp)

    def offset_of(i):
        odd = lax.rem(i, 2)
        return odd * ((i + 1) // 2) + (1 - odd) * lax.rem(n_ep - i // 2, n_ep)

    def ep_peer(i):
        return lax.rem(p + offset_of(i), n_ep)

    def wait_bytes(region, sem):
        pltpu.make_async_copy(region, region, sem).wait()

    def to_tp(src_of, dst_of, sems):
        def step(k, carry):
            q = tp_peer(k)
            pltpu.make_async_remote_copy(
                src_of(q), dst_of(k), sems.at[0], sems.at[1], device_id=(p, q), device_id_type=MESH
            ).start()
            return carry

        lax.fori_loop(1, n_tp, step, 0)

    pairs = [
        (tokens_h, tokens), (gain1_h, gain1), (wq_h, wq), (wk_h, wk), (wl_h, wl), (wd_h, wd), (bias_h, bias),
        (wv_h, wv), (wo_h, wo), (ids_h, ids), (rw_h, rw), (hgain_h, hgain), (state_h, state), (wout_h, wout),
        (gain2_h, gain2), (sg_h, sg), (su_h, su), (sd_h, sd), (eg_h, eg), (eu_h, eu), (ed_h, ed),
    ]
    loads = {}
    for number, (src, dst) in enumerate(pairs):
        loads[id(dst)] = (src, dst, in_sem.at[number])

    def ready(*refs):
        for ref in refs:
            pltpu.make_async_copy(*loads[id(ref)]).wait()

    barrier = pltpu.get_barrier_semaphore()

    def greet_tp(k, carry):
        pl.semaphore_signal(barrier, inc=1, device_id=(p, tp_peer(k)), device_id_type=MESH)
        return carry

    def greet_ep(i, carry):
        pl.semaphore_signal(barrier, inc=1, device_id=(lax.rem(p + i, n_ep), t), device_id_type=MESH)
        return carry

    lax.fori_loop(1, n_ep, greet_ep, 0)
    lax.fori_loop(1, n_tp, greet_tp, 0)
    for _, dst in pairs:
        pltpu.make_async_copy(*loads[id(dst)]).start()

    ready(tokens)
    ready(gain1)
    squares = jnp.zeros((seqs, LANES), F32)
    for j in range(blocks):
        x = tokens[:, j * LANES : (j + 1) * LANES].astype(F32)
        squares += x * x
    inverse = lax.rsqrt(jnp.sum(squares, axis=1, keepdims=True) / width + EPSILON)
    gains = gain1[...].astype(F32)
    for j in range(blocks):
        x = tokens[:, j * LANES : (j + 1) * LANES].astype(F32)
        normed[:, j * LANES : (j + 1) * LANES] = (x * inverse * gains[j : j + 1, :]).astype(BF16)
    own_normed[...] = normed[:, own_cols]

    ready(wq)
    ready(wk)
    query_part = dot(own_normed[...], wq[...]).astype(BF16)
    key_part = dot(own_normed[...], wk[...]).astype(BF16)
    for h in range(heads):
        a_send[h, :, :dk] = query_part[:, h * dk : (h + 1) * dk]
        a_send[h, :, dk:] = key_part[:, h * dk : (h + 1) * dk]

    pl.semaphore_wait(barrier, n_ep + n_tp - 2)
    to_tp(lambda q: a_send.at[q // per_head], lambda k: a_recv.at[k - 1], a_sem)

    ready(wl)
    ready(wd)
    ready(bias)
    lowrank = dot_t(normed[...], wl[...]).astype(BF16)
    head_cols = pl.ds(pl.multiple_of(head * dk, dk), dk)
    decay_in = dot(lowrank, wd[:, head_cols])
    bias_all = bias[...]
    bias_row = lax.broadcasted_iota(jnp.int32, bias_all.shape, 0)
    bias_cols = [
        jnp.sum(jnp.where(bias_row == head * (dk // LANES) + m, bias_all, 0.0), axis=0, keepdims=True)
        for m in range(dk // LANES)
    ]
    decay_in = decay_in + jnp.concatenate(bias_cols, axis=1)
    log_decay = -(jnp.maximum(-decay_in, 0.0) + jnp.log1p(jnp.exp(-jnp.abs(decay_in)))) / 16.0
    decay = jnp.exp(log_decay)
    ready(wv)
    ready(wo)
    value = dot(normed[...], wv[...]).astype(BF16)
    out_gate = dot(normed[...], wo[...]).astype(BF16)
    ready(hgain)
    gate = hgain[...].astype(F32) * silu(out_gate.astype(F32))

    ready(ids)
    ready(rw)
    row = lax.broadcasted_iota(jnp.int32, (slots, seqs), 0)
    slot = row // 2
    odd = slot % 2
    offset = odd * ((slot + 1) // 2) + (1 - odd) * ((n_ep - slot // 2) % n_ep)
    expert = (p + offset) % n_ep
    route_ids = ids[...]
    route_weights = rw[...]
    named = jnp.zeros((slots, seqs), F32)
    weight = jnp.zeros((slots, seqs), F32)
    for j in range(route_ids.shape[0]):
        hit = route_ids[j : j + 1, :] == expert
        named = named + jnp.where(hit, 1.0, 0.0)
        weight = weight + jnp.where(hit, route_weights[j : j + 1, :], 0.0)
    earlier = (
        lax.broadcasted_iota(jnp.int32, (seqs, seqs), 0) < lax.broadcasted_iota(jnp.int32, (seqs, seqs), 1)
    )
    rank = dot(named.astype(BF16), jnp.where(earlier, 1.0, 0.0).astype(BF16))
    chosen = jnp.where(rank == (row % 2).astype(F32), named, 0.0)
    placing = chosen.astype(BF16)
    weight = jnp.concatenate([weight * chosen, jnp.zeros((slots, LANES - seqs), F32)], axis=1).T[:seqs]
    weight_hi = weight.astype(BF16)
    weight_lo = (weight - weight_hi.astype(F32)).astype(BF16)

    ready(state)
    ready(wout)

    wait_bytes(a_recv, a_sem.at[1])
    total = a_send[head].astype(F32)
    for k in range(n_tp - 1):
        total = total + a_recv[k].astype(F32)
    query = total[:, :dk].astype(BF16)
    key = total[:, dk:].astype(BF16)
    query_f, key_f = query.astype(F32), key.astype(F32)

    decayed = query_f * decay
    decayed_hi = decayed.astype(BF16)
    decayed_lo = (decayed - decayed_hi.astype(F32)).astype(BF16)
    both = jnp.concatenate([decayed_hi, decayed_lo], axis=0)
    row = lax.broadcasted_iota(jnp.int32, (seqs, vc), 0)
    read = jnp.sum(query_f * key_f, axis=1, keepdims=True) * value.astype(F32)
    for b in range(seqs):
        got = dot(both, state[b])
        read = read + jnp.where(row == b, got[:seqs] + got[seqs:], 0.0)
    read = read * dk**-0.5
    own_squares = jnp.sum(read * read, axis=1, keepdims=True)
    mixed = (read * gate).astype(BF16)
    part = dot(mixed, wout[...]).astype(BF16)
    sq_hi = own_squares.astype(BF16).astype(F32)
    sq_lo = (own_squares - sq_hi).astype(BF16).astype(F32)
    first_lanes = lax.broadcasted_iota(jnp.int32, (seqs, LANES), 1)
    carried_squares = jnp.where(first_lanes == 0, sq_hi, jnp.where(first_lanes == 1, sq_lo, 0.0)).astype(BF16)
    for q in range(n_tp):
        b_send[q, :seqs, :] = part[:, q * LANES : (q + 1) * LANES]
        b_send[q, seqs:, :] = carried_squares
    to_tp(lambda q: b_send.at[q], lambda k: b_recv.at[t], b_sem)
    b_recv[t] = b_send[t]

    padded = jnp.concatenate(
        [
            key_f,
            decay.astype(BF16).astype(F32),
            (decay - decay.astype(BF16).astype(F32)),
            jnp.zeros((LANES - 3 * seqs, dk), F32),
        ],
        axis=0,
    )
    columns = padded.T.astype(BF16)
    value_rows = jnp.concatenate([value.astype(F32), jnp.zeros((LANES - seqs, vc), F32)], axis=0)
    wide_row = lax.broadcasted_iota(jnp.int32, (LANES, vc), 0)
    ready(gain2)
    gains = gain2[...].astype(F32)

    wait_bytes(b_recv.at[pl.ds(0, n_tp - 1)], b_sem.at[1])
    second = tokens[:, own_cols].astype(F32)
    for h in range(heads):
        parts = jnp.zeros((seqs, LANES), F32)
        sums = jnp.zeros((seqs, LANES), F32)
        for q in range(h * per_head, (h + 1) * per_head):
            got = b_recv[q].astype(F32)
            parts = parts + got[:seqs]
            sums = sums + got[seqs:]
        scale = lax.rsqrt(jnp.sum(sums, axis=1, keepdims=True) / head_width + EPSILON)
        second = second + scale * parts
    second = second.astype(BF16)
    c_send[...] = second

    d_send[...] = dot(placing, second).reshape(n_ep, 2, LANES).astype(BF16)

    def dispatch(step, carry):
        i = n_ep - 1 - step
        pltpu.make_async_remote_copy(
            d_send.at[i], d_recv.at[i], d_sem.at[0], d_sem.at[1 + i // n_chunk],
            device_id=(ep_peer(i), t), device_id_type=MESH,
        ).start()
        return carry

    lax.fori_loop(0, n_ep - 1, dispatch, 0)
    to_tp(lambda q: c_send, lambda k: c_recv.at[t], c_sem)
    c_recv[t] = second
    d_recv[0] = d_send[0]

    def update(b, carry):
        right = jnp.concatenate(
            [
                jnp.where(wide_row == b, value_rows, 0.0),
                jnp.where((wide_row == seqs + b) | (wide_row == 2 * seqs + b), 1.0, 0.0),
            ],
            axis=1,
        ).astype(BF16)
        made = dot(columns, right)
        newstate[b] = (made[:, vc:] * state[b].astype(F32) + made[:, :vc]).astype(BF16)
        pltpu.make_async_copy(newstate.at[b], newstate_h.at[b], out_sem.at[1]).start()
        return carry

    lax.fori_loop(0, seqs, update, 0)

    def normalise(pieces, result, count):
        squares = jnp.zeros((count, LANES), F32)
        for j in range(blocks):
            x = pieces(j).astype(F32)
            squares = squares + x * x
        inverse = lax.rsqrt(jnp.sum(squares, axis=1, keepdims=True) / width + EPSILON)
        for j in range(blocks):
            x = pieces(j).astype(F32)
            result[:, j * LANES : (j + 1) * LANES] = (x * inverse * gains[j : j + 1, :]).astype(BF16)

    wait_bytes(c_recv.at[pl.ds(0, n_tp - 1)], c_sem.at[1])
    normalise(lambda j: c_recv[j], n2, seqs)
    ready(sg)
    ready(su)
    ready(sd)
    hidden = (silu(dot_t(n2[...], sg[...])) * dot_t(n2[...], su[...])).astype(BF16)
    down = dot(hidden, sd[...]).astype(BF16)
    for q in range(n_tp):
        s_send[q] = down[:, q * LANES : (q + 1) * LANES]
    to_tp(lambda q: s_send.at[q], lambda k: s_recv.at[k - 1], s_sem)
    ready(eg)
    ready(eu)
    ready(ed)

    def gather(c):
        first = 1 if c == 0 else c * n_chunk
        wait_bytes(d_recv.at[pl.ds(first, (c + 1) * n_chunk - first)], d_sem.at[1 + c])
        block = d_recv[c * n_chunk : (c + 1) * n_chunk].astype(F32).reshape(rows, LANES).astype(BF16)
        e_send[c] = block
        to_tp(lambda q: e_send.at[c], lambda k: e_recv.at[c, t], e_sem.at[c])
        e_recv[c, t] = block

    def experts(c):
        wait_bytes(e_recv.at[c, pl.ds(0, n_tp - 1)], e_sem.at[c, 1])
        normalise(lambda j: e_recv[c, j], xn, rows)
        hidden = (silu(dot_t(xn[...], eg[0])) * dot_t(xn[...], eu[0])).astype(BF16)
        down = dot(hidden, ed[0]).astype(BF16)
        for q in range(n_tp):
            g_send[c, q] = down[:, q * LANES : (q + 1) * LANES]
        to_tp(lambda q: g_send.at[c, q], lambda k: g_recv.at[c, k - 1], g_sem.at[c])

    def give_back(c):
        wait_bytes(g_recv.at[c], g_sem.at[c, 1])
        total = g_send[c, t].astype(F32)
        for k in range(n_tp - 1):
            total = total + g_recv[c, k].astype(F32)
        h_send[c * n_chunk : (c + 1) * n_chunk] = total.reshape(n_chunk, 2, LANES).astype(BF16)
        first = 1 if c == 0 else c * n_chunk

        def step(s, carry):
            i = (c + 1) * n_chunk - 1 - s
            back = lax.rem(p + n_ep - offset_of(i), n_ep)
            pltpu.make_async_remote_copy(
                h_send.at[i], h_recv.at[i], h_sem.at[0], h_sem.at[1],
                device_id=(back, t), device_id_type=MESH,
            ).start()
            return carry

        lax.fori_loop(0, (c + 1) * n_chunk - first, step, 0)
        if c == 0:
            h_recv[0] = h_send[0]

    for c in range(chunks):
        gather(c)
        if c >= 1:
            experts(c - 1)
        if c >= 2:
            give_back(c - 2)
    if chunks >= 2:
        give_back(chunks - 2)
    experts(chunks - 1)
    give_back(chunks - 1)

    wait_bytes(s_recv, s_sem.at[1])
    total = s_send[t].astype(F32)
    for k in range(n_tp - 1):
        total = total + s_recv[k].astype(F32)
    total = total + c_send[...].astype(F32)
    wait_bytes(a_recv, a_sem.at[0])
    wait_bytes(b_recv.at[pl.ds(0, n_tp - 1)], b_sem.at[0])
    wait_bytes(c_recv.at[pl.ds(0, n_tp - 1)], c_sem.at[0])
    wait_bytes(s_recv, s_sem.at[0])
    wait_bytes(d_recv.at[pl.ds(1, n_ep - 1)], d_sem.at[0])
    for c in range(chunks):
        wait_bytes(e_recv.at[c, pl.ds(0, n_tp - 1)], e_sem.at[c, 0])
        wait_bytes(g_recv.at[c], g_sem.at[c, 0])
    wait_bytes(newstate, out_sem.at[1])

    wait_bytes(h_recv.at[pl.ds(1, n_ep - 1)], h_sem.at[1])
    returned = h_recv[...].astype(F32).reshape(slots, LANES).astype(BF16)
    total = total + dot(weight_hi, returned) + dot(weight_lo, returned)
    out[...] = total.astype(BF16)
    result = pltpu.make_async_copy(out, out_h, out_sem.at[0])
    result.start()
    wait_bytes(h_recv.at[pl.ds(1, n_ep - 1)], h_sem.at[0])
    result.wait()


def body(n_ep, n_tp, *args):
    (
        tokens, old_state, first_gain, query_weight, key_weight, value_weight, outgate_weight, lowrank_weight,
        decay_weight, decay_bias, head_gain, output_weight, second_gain, expert_gate, expert_up, expert_down,
        shared_gate, shared_up, shared_down, route_ids, route_weights,
    ) = args
    seqs, width = tokens.shape
    dk = old_state.shape[1]
    heads = decay_weight.shape[1] // dk
    chunks = CHUNKS
    blocks = width // LANES
    operands = [
        tokens, old_state, first_gain.reshape(blocks, LANES), query_weight, key_weight, value_weight, outgate_weight,
        lowrank_weight.T, decay_weight, decay_bias.reshape(-1, LANES), head_gain.reshape(1, -1), output_weight,
        second_gain.reshape(blocks, LANES), expert_gate.swapaxes(1, 2), expert_up.swapaxes(1, 2), expert_down,
        shared_gate.T, shared_up.T, shared_down, route_ids.T, route_weights.T,
    ]
    rows = 2 * n_ep // chunks
    vmem = lambda shape, dtype=BF16: pltpu.VMEM(shape, dtype)
    dma = pltpu.SemaphoreType.DMA
    scratch = [vmem(x.shape, x.dtype) for x in operands]
    scratch += [
        vmem((seqs, width)),
        vmem((seqs, LANES)),
        vmem((heads, seqs, 2 * dk)),
        vmem((n_tp - 1, seqs, 2 * dk)),
        vmem((n_tp, 2 * seqs, LANES)),
        vmem((n_tp, 2 * seqs, LANES)),
        vmem((seqs, LANES)),
        vmem((n_tp, seqs, LANES)),
        vmem((seqs, width)),
        vmem((n_tp, seqs, LANES)),
        vmem((n_tp - 1, seqs, LANES)),
        vmem((n_ep, 2, LANES)),
        vmem((n_ep, 2, LANES)),
        vmem((chunks, rows, LANES)),
        vmem((chunks, n_tp, rows, LANES)),
        vmem((rows, width)),
        vmem((chunks, n_tp, rows, LANES)),
        vmem((chunks, n_tp - 1, rows, LANES)),
        vmem((n_ep, 2, LANES)),
        vmem((n_ep, 2, LANES)),
        vmem(old_state.shape),
        vmem((seqs, LANES)),
        dma((len(operands),)),
        dma((2,)),
        dma((2,)),
        dma((2,)),
        dma((2,)),
        dma((2,)),
        dma((1 + chunks,)),
        dma((chunks, 2)),
        dma((chunks, 2)),
        dma((2,)),
    ]
    return pl.pallas_call(
        functools.partial(kernel, (n_ep, n_tp, heads, chunks)),
        out_shape=(
            jax.ShapeDtypeStruct((seqs, LANES), BF16),
            jax.ShapeDtypeStruct(old_state.shape, BF16),
        ),
        in_specs=[pl.BlockSpec(memory_space=pltpu.HBM)] * len(operands),
        out_specs=(pl.BlockSpec(memory_space=pl.ANY), pl.BlockSpec(memory_space=pl.ANY)),
        scratch_shapes=scratch,
        compiler_params=pltpu.CompilerParams(
            collective_id=0, has_side_effects=True
        ),
    )(*operands)


def solution(mesh):
    return jax.shard_map(
        functools.partial(body, mesh.shape["ep"], mesh.shape["tp"]),
        mesh=mesh,
        in_specs=(
            P("ep", None),
            P("ep", None, "tp"),
            P(),
            P("tp", None),
            P("tp", None),
            P(None, "tp"),
            P(None, "tp"),
            P(),
            P(),
            P(),
            P("tp"),
            P("tp", None),
            P(),
            P("ep", None, "tp"),
            P("ep", None, "tp"),
            P("ep", "tp", None),
            P(None, "tp"),
            P(None, "tp"),
            P("tp", None),
            P("ep", None),
            P("ep", None),
        ),
        out_specs=(P("ep", "tp"), P("ep", None, "tp")),
        check_vma=False,
    )
```

time: 207 us -> 89.7 us (0.43)
  Pallas kernels: 0 us -> 85.3 us
  blocking collectives: 81 us -> 0 us
  waiting for transfers between devices: 69.5 us -> 0 us
  starting transfers between devices: 29.7 us -> 0 us
  matrix products: 8.84 us -> 0 us
  other arithmetic: 6.72 us -> 0 us
  local copies, waits for them, and re-layouts: 8.95 us -> 3.57 us
    pallas_call x0 -> x1, Pallas kernels: none -> 85.3 us  [body(): pl.pallas_call(functools.partial(kernel, (n_ep, n_tp, heads, chunks)), ou...]
    all_to_all x7 -> x0, waiting for transfers between devices: 69.5 us -> none  [the longest x4 37 us: from_everyone(): lax.all_to_all(jnp.broadcast_to(value[None], (devices, *value.shape)), ax...]
    all_to_all x2 -> x0, blocking collectives: 67.3 us -> none  [the longest x1 60.7 us: body(): lax.all_to_all(dispatched, EP, split_axis=0, concat_axis=0, tiled=True)]
    all_to_all x7 -> x0, starting transfers between devices: 29.7 us -> none  [the longest x4 18.6 us: from_everyone(): lax.all_to_all(jnp.broadcast_to(value[None], (devices, *value.shape)), ax...]
    psum x2 -> x0, blocking collectives: 13.7 us -> none  [by_axis(): value = lax.psum(value, axis)]
    dot_general x11 -> x0, matrix products: 8.84 us -> none  [the longest x8 4.75 us: project(): return jnp.dot(left_side, right_side, preferred_element_type=jnp.float32)]
    convert_element_type x9 -> x0, other arithmetic: 4.53 us -> none  [the longest x1 2.04 us: body(): new_state = carried.astype(jnp.bfloat16)]
    broadcast_in_dim x5 -> x0, local copies, waits for them, and re-layouts: 4.02 us -> none  [the longest x4 4.01 us: from_everyone(): jnp.broadcast_to(value[None], (devices, *value.shape))]
  transfers between devices with their start and end apart: 7 -> 0, of which waited for: 7 -> 0; matrix products, arithmetic and copies ran while one was open for 4% -> 0% of each run, Pallas kernels for 0% -> 0%
where the time goes in v1:
time: 89.7 us; the launch traced here: 89.5 us
  Pallas kernels  85.3 us (95%)
  local copies, waits for them, and re-layouts  3.57 us (4%)
    pallas_call x1, Pallas kernels, body(): pl.pallas_call(functools.partial(kernel, (n_ep, n_tp, heads, chunks)), ou...  85.3 us
    unnamed x2, local copies, waits for them, and re-layouts  3.57 us

profile of v1, /device:TPU:1, one launch (start us, length us, event | category | flops | bytes accessed | tf_op | source)
XLA Modules:
  0.0 89.5 jit_solution(16868356232965195807)
XLA Ops:
  0.6 85.3 %shard_map.212 = (bf16[16,128]{1,0:T(8,128)(2,1)}, bf16[16,256,128]{2,1,0:T(8,128)(2,1)}) custom-call(bf16[16,2048]{1,0:T(8,128)(2,1)} %tokens_h.1, bf16[16,256,128]{2,1,0:T(8,128)(2,1)} %state_h.1, bf16[16,128]{1,0:T(8,128)(2,1)} %bitcast.16, bf16[128,1024]{1,0:T(8,128)(2,1)} %wq_h.1, bf16[128,1024]{1,0:T(8,128)(2,1)} %wk_h.1, bf16[2048,128]{1,0:T(8,128)(2,1)} %wv_h.1, ...), custom_call_target="tpu_custom_call" | custom-call | tf_op jit(solution)/shard_map/pallas_call | solution.py:422
  86.0 1.3 %copy.25 = bf16[16,128]{1,0:T(8,128)(2,1)} copy(bf16[16,128]{1,0:T(8,128)(2,1)} %get-tuple-element.4) | data formatting | bytes 8192
  87.2 2.3 %copy.26 = bf16[16,256,128]{2,1,0:T(8,128)(2,1)} copy(bf16[16,256,128]{2,1,0:T(8,128)(2,1)} %get-tuple-element.5) | data formatting | bytes 2097152

commit v2 on v1

--- a/solution.py
+++ b/solution.py
@@ -31,11 +31,11 @@
     sizes,
     tokens_h, state_h, gain1_h, wq_h, wk_h, wv_h, wo_h, wl_h, wd_h, bias_h, hgain_h, wout_h, gain2_h,
     eg_h, eu_h, ed_h, sg_h, su_h, sd_h, ids_h, rw_h,
-    out_h, newstate_h,
+    out, newstate,
     tokens, state, gain1, wq, wk, wv, wo, wl, wd, bias, hgain, wout, gain2, eg, eu, ed, sg, su, sd, ids, rw,
     normed, own_normed, a_send, a_recv, b_send, b_recv, c_send, c_recv, n2, s_send, s_recv,
-    d_send, d_recv, e_send, e_recv, xn, g_send, g_recv, h_send, h_recv, newstate, out,
-    in_sem, out_sem, a_sem, b_sem, c_sem, s_sem, d_sem, e_sem, g_sem, h_sem,
+    d_send, d_recv, e_send, e_recv, xn, g_send, g_recv, h_send, h_recv,
+    in_sem, a_sem, b_sem, c_sem, s_sem, d_sem, e_sem, g_sem, h_sem, z_sem,
 ):
     n_ep, n_tp, heads, chunks = sizes
     seqs, width = tokens.shape
@@ -88,19 +88,39 @@
             pltpu.make_async_copy(*loads[id(ref)]).wait()
 
     barrier = pltpu.get_barrier_semaphore()
+    n_z = n_ep // 2
+    z, core = p // 2, lax.rem(p, 2)
+
+    def chip(d):
+        return lax.rem(z + n_z + d, n_z)
 
     def greet_tp(k, carry):
         pl.semaphore_signal(barrier, inc=1, device_id=(p, tp_peer(k)), device_id_type=MESH)
         return carry
 
-    def greet_ep(i, carry):
-        pl.semaphore_signal(barrier, inc=1, device_id=(lax.rem(p + i, n_ep), t), device_id_type=MESH)
-        return carry
-
-    lax.fori_loop(1, n_ep, greet_ep, 0)
+    early = (tokens, gain1, wq, wk)
+    for ref in early:
+        pltpu.make_async_copy(*loads[id(ref)]).start()
+    near = [2 * z + 1 - core] + [2 * chip(d) + c for d in (1, -1) for c in (0, 1)]
+    for q in near:
+        pl.semaphore_signal(barrier, inc=1, device_id=(q, t), device_id_type=MESH)
     lax.fori_loop(1, n_tp, greet_tp, 0)
     for _, dst in pairs:
-        pltpu.make_async_copy(*loads[id(dst)]).start()
+        if all(dst is not ref for ref in early):
+            pltpu.make_async_copy(*loads[id(dst)]).start()
+
+    rounds = []
+    while 2 ** len(rounds) < n_z // 2:
+        rounds.append(2 ** len(rounds))
+
+    def tell(r):
+        if r < len(rounds):
+            for d in (rounds[r], -rounds[r]):
+                pl.semaphore_signal(z_sem.at[r], inc=1, device_id=(2 * chip(d) + core, t), device_id_type=MESH)
+
+    def hear(r):
+        if r < len(rounds):
+            pl.semaphore_wait(z_sem.at[r], 2)
 
     ready(tokens)
     ready(gain1)
@@ -123,8 +143,9 @@
         a_send[h, :, :dk] = query_part[:, h * dk : (h + 1) * dk]
         a_send[h, :, dk:] = key_part[:, h * dk : (h + 1) * dk]
 
-    pl.semaphore_wait(barrier, n_ep + n_tp - 2)
+    pl.semaphore_wait(barrier, n_tp - 1 + len(near))
     to_tp(lambda q: a_send.at[q // per_head], lambda k: a_recv.at[k - 1], a_sem)
+    tell(0)
 
     ready(wl)
     ready(wd)
@@ -176,7 +197,14 @@
     ready(state)
     ready(wout)
 
+    hear(0)
+    tell(1)
+    hear(1)
+    tell(2)
+
     wait_bytes(a_recv, a_sem.at[1])
+    hear(2)
+    tell(3)
     total = a_send[head].astype(F32)
     for k in range(n_tp - 1):
         total = total + a_recv[k].astype(F32)
@@ -222,6 +250,20 @@
     ready(gain2)
     gains = gain2[...].astype(F32)
 
+    def update(b, carry):
+        right = jnp.concatenate(
+            [
+                jnp.where(wide_row == b, value_rows, 0.0),
+                jnp.where((wide_row == seqs + b) | (wide_row == 2 * seqs + b), 1.0, 0.0),
+            ],
+            axis=1,
+        ).astype(BF16)
+        made = dot(columns, right)
+        newstate[b] = (made[:, vc:] * state[b].astype(F32) + made[:, :vc]).astype(BF16)
+        return carry
+
+    lax.fori_loop(0, seqs, update, 0)
+
     wait_bytes(b_recv.at[pl.ds(0, n_tp - 1)], b_sem.at[1])
     second = tokens[:, own_cols].astype(F32)
     for h in range(heads):
@@ -238,6 +280,8 @@
 
     d_send[...] = dot(placing, second).reshape(n_ep, 2, LANES).astype(BF16)
 
+    hear(3)
+
     def dispatch(step, carry):
         i = n_ep - 1 - step
         pltpu.make_async_remote_copy(
@@ -250,21 +294,6 @@
     to_tp(lambda q: c_send, lambda k: c_recv.at[t], c_sem)
     c_recv[t] = second
     d_recv[0] = d_send[0]
-
-    def update(b, carry):
-        right = jnp.concatenate(
-            [
-                jnp.where(wide_row == b, value_rows, 0.0),
-                jnp.where((wide_row == seqs + b) | (wide_row == 2 * seqs + b), 1.0, 0.0),
-            ],
-            axis=1,
-        ).astype(BF16)
-        made = dot(columns, right)
-        newstate[b] = (made[:, vc:] * state[b].astype(F32) + made[:, :vc]).astype(BF16)
-        pltpu.make_async_copy(newstate.at[b], newstate_h.at[b], out_sem.at[1]).start()
-        return carry
-
-    lax.fori_loop(0, seqs, update, 0)
 
     def normalise(pieces, result, count):
         squares = jnp.zeros((count, LANES), F32)
@@ -332,12 +361,9 @@
         gather(c)
         if c >= 1:
             experts(c - 1)
-        if c >= 2:
-            give_back(c - 2)
-    if chunks >= 2:
-        give_back(chunks - 2)
     experts(chunks - 1)
-    give_back(chunks - 1)
+    for c in range(chunks):
+        give_back(c)
 
     wait_bytes(s_recv, s_sem.at[1])
     total = s_send[t].astype(F32)
@@ -352,16 +378,12 @@
     for c in range(chunks):
         wait_bytes(e_recv.at[c, pl.ds(0, n_tp - 1)], e_sem.at[c, 0])
         wait_bytes(g_recv.at[c], g_sem.at[c, 0])
-    wait_bytes(newstate, out_sem.at[1])
 
     wait_bytes(h_recv.at[pl.ds(1, n_ep - 1)], h_sem.at[1])
     returned = h_recv[...].astype(F32).reshape(slots, LANES).astype(BF16)
     total = total + dot(weight_hi, returned) + dot(weight_lo, returned)
     out[...] = total.astype(BF16)
-    result = pltpu.make_async_copy(out, out_h, out_sem.at[0])
-    result.start()
     wait_bytes(h_recv.at[pl.ds(1, n_ep - 1)], h_sem.at[0])
-    result.wait()
 
 
 def body(n_ep, n_tp, *args):
@@ -406,10 +428,7 @@
         vmem((chunks, n_tp - 1, rows, LANES)),
         vmem((n_ep, 2, LANES)),
         vmem((n_ep, 2, LANES)),
-        vmem(old_state.shape),
-        vmem((seqs, LANES)),
         dma((len(operands),)),
-        dma((2,)),
         dma((2,)),
         dma((2,)),
         dma((2,)),
@@ -418,15 +437,16 @@
         dma((chunks, 2)),
         dma((chunks, 2)),
         dma((2,)),
+        pltpu.SemaphoreType.REGULAR((4,)),
     ]
     return pl.pallas_call(
         functools.partial(kernel, (n_ep, n_tp, heads, chunks)),
         out_shape=(
-            jax.ShapeDtypeStruct((seqs, LANES), BF16),
-            jax.ShapeDtypeStruct(old_state.shape, BF16),
+            pltpu.VMEM((seqs, LANES), BF16),
+            pltpu.VMEM(old_state.shape, BF16),
         ),
         in_specs=[pl.BlockSpec(memory_space=pltpu.HBM)] * len(operands),
-        out_specs=(pl.BlockSpec(memory_space=pl.ANY), pl.BlockSpec(memory_space=pl.ANY)),
+        out_specs=(pl.BlockSpec(memory_space=pltpu.VMEM), pl.BlockSpec(memory_space=pltpu.VMEM)),
         scratch_shapes=scratch,
         compiler_params=pltpu.CompilerParams(
             collective_id=0, has_side_effects=True

time: 89.7 us -> 77.9 us (0.87)
  Pallas kernels: 85.3 us -> 75.5 us
  local copies, waits for them, and re-layouts: 3.57 us -> 1.56 us
    pallas_call x1, Pallas kernels: 85.3 us -> 75.5 us  [body(): pl.pallas_call(functools.partial(kernel, (n_ep, n_tp, heads, chunks)), ou...]
    unnamed x2, local copies, waits for them, and re-layouts: 3.57 us -> 1.56 us
where the time goes in v2:
time: 77.9 us; the launch traced here: 77.7 us
  Pallas kernels  75.5 us (97%)
  local copies, waits for them, and re-layouts  1.56 us (2%)
    pallas_call x1, Pallas kernels, body(): pl.pallas_call(functools.partial(kernel, (n_ep, n_tp, heads, chunks)), ou...  75.5 us
    unnamed x2, local copies, waits for them, and re-layouts  1.56 us

profile of v2, /device:TPU:1, one launch (start us, length us, event | category | flops | bytes accessed | tf_op | source)
XLA Modules:
  0.0 77.7 jit_solution(4525788671761570134)
XLA Ops:
  0.6 75.5 %shard_map.212 = (bf16[16,128]{1,0:T(8,128)(2,1)S(1)}, bf16[16,256,128]{2,1,0:T(8,128)(2,1)S(1)}) custom-call(bf16[16,2048]{1,0:T(8,128)(2,1)} %tokens_h.1, bf16[16,256,128]{2,1,0:T(8,128)(2,1)} %state_h.1, bf16[16,128]{1,0:T(8,128)(2,1)} %bitcast.16, bf16[128,1024]{1,0:T(8,128)(2,1)} %wq_h.1, bf16[128,1024]{1,0:T(8,128)(2,1)} %wk_h.1, ...), custom_call_target="tpu_custom_call" | custom-call | tf_op jit(solution)/shard_map/pallas_call | solution.py:442
  76.2 0.6 copy.25
  76.8 1.0 %copy.26 = bf16[16,256,128]{2,1,0:T(8,128)(2,1)} copy(bf16[16,256,128]{2,1,0:T(8,128)(2,1)S(1)} %get-tuple-element.3) | data formatting | bytes 2097152

commit v3 on v2

--- a/solution.py
+++ b/solution.py
@@ -51,9 +51,6 @@
     head = t // per_head
     own_cols = pl.ds(pl.multiple_of(t * LANES, LANES), LANES)
 
-    def tp_peer(k):
-        return lax.rem(t + k, n_tp)
-
     def offset_of(i):
         odd = lax.rem(i, 2)
         return odd * ((i + 1) // 2) + (1 - odd) * lax.rem(n_ep - i // 2, n_ep)
@@ -64,15 +61,33 @@
     def wait_bytes(region, sem):
         pltpu.make_async_copy(region, region, sem).wait()
 
+    side = 4 if n_tp == 16 else 1
+    hops = [0, 1, 2, 1]
+    steps = [(dy, dx) for dy in range(side) for dx in range(side)][1:] if side > 1 else range(1, n_tp)
+    steps = sorted(steps, key=lambda s: -(hops[s[0]] + hops[s[1]])) if side > 1 else steps
+
+    def partner(s):
+        if side == 1:
+            return lax.rem(t + s, n_tp)
+        return lax.rem(t // side + s[0], side) * side + lax.rem(t + s[1], side)
+
+    tp_partners = [partner(s) for s in steps]
+
     def to_tp(src_of, dst_of, sems):
-        def step(k, carry):
-            q = tp_peer(k)
+        for k, q in enumerate(tp_partners):
             pltpu.make_async_remote_copy(
                 src_of(q), dst_of(k), sems.at[0], sems.at[1], device_id=(p, q), device_id_type=MESH
             ).start()
+
+    def unrolled(count, step):
+        width_of = next(u for u in (7, 5, 4, 3, 2, 1) if count % u == 0)
+
+        def some(j, carry):
+            for u in range(width_of):
+                step(j * width_of + u)
             return carry
 
-        lax.fori_loop(1, n_tp, step, 0)
+        lax.fori_loop(0, count // width_of, some, 0)
 
     pairs = [
         (tokens_h, tokens), (gain1_h, gain1), (wq_h, wq), (wk_h, wk), (wl_h, wl), (wd_h, wd), (bias_h, bias),
@@ -94,20 +109,15 @@
     def chip(d):
         return lax.rem(z + n_z + d, n_z)
 
-    def greet_tp(k, carry):
-        pl.semaphore_signal(barrier, inc=1, device_id=(p, tp_peer(k)), device_id_type=MESH)
-        return carry
-
-    early = (tokens, gain1, wq, wk)
-    for ref in early:
-        pltpu.make_async_copy(*loads[id(ref)]).start()
     near = [2 * z + 1 - core] + [2 * chip(d) + c for d in (1, -1) for c in (0, 1)]
+    for _, dst in pairs[:2]:
+        pltpu.make_async_copy(*loads[id(dst)]).start()
     for q in near:
         pl.semaphore_signal(barrier, inc=1, device_id=(q, t), device_id_type=MESH)
-    lax.fori_loop(1, n_tp, greet_tp, 0)
-    for _, dst in pairs:
-        if all(dst is not ref for ref in early):
-            pltpu.make_async_copy(*loads[id(dst)]).start()
+    for q in tp_partners:
+        pl.semaphore_signal(barrier, inc=1, device_id=(p, q), device_id_type=MESH)
+    for _, dst in pairs[2:12]:
+        pltpu.make_async_copy(*loads[id(dst)]).start()
 
     rounds = []
     while 2 ** len(rounds) < n_z // 2:
@@ -135,6 +145,9 @@
         normed[:, j * LANES : (j + 1) * LANES] = (x * inverse * gains[j : j + 1, :]).astype(BF16)
     own_normed[...] = normed[:, own_cols]
 
+    pl.semaphore_wait(barrier, n_tp - 1 + len(near))
+    tell(0)
+
     ready(wq)
     ready(wk)
     query_part = dot(own_normed[...], wq[...]).astype(BF16)
@@ -143,9 +156,10 @@
         a_send[h, :, :dk] = query_part[:, h * dk : (h + 1) * dk]
         a_send[h, :, dk:] = key_part[:, h * dk : (h + 1) * dk]
 
-    pl.semaphore_wait(barrier, n_tp - 1 + len(near))
-    to_tp(lambda q: a_send.at[q // per_head], lambda k: a_recv.at[k - 1], a_sem)
-    tell(0)
+    to_tp(lambda q: a_send.at[q // per_head], lambda k: a_recv.at[k], a_sem)
+
+    for _, dst in pairs[12:]:
+        pltpu.make_async_copy(*loads[id(dst)]).start()
 
     ready(wl)
     ready(wd)
@@ -201,10 +215,10 @@
     tell(1)
     hear(1)
     tell(2)
-
-    wait_bytes(a_recv, a_sem.at[1])
     hear(2)
     tell(3)
+
+    wait_bytes(a_recv, a_sem.at[1])
     total = a_send[head].astype(F32)
     for k in range(n_tp - 1):
         total = total + a_recv[k].astype(F32)
@@ -282,15 +296,14 @@
 
     hear(3)
 
-    def dispatch(step, carry):
+    def dispatch(step):
         i = n_ep - 1 - step
         pltpu.make_async_remote_copy(
             d_send.at[i], d_recv.at[i], d_sem.at[0], d_sem.at[1 + i // n_chunk],
             device_id=(ep_peer(i), t), device_id_type=MESH,
         ).start()
-        return carry
-
-    lax.fori_loop(0, n_ep - 1, dispatch, 0)
+
+    unrolled(n_ep - 1, dispatch)
     to_tp(lambda q: c_send, lambda k: c_recv.at[t], c_sem)
     c_recv[t] = second
     d_recv[0] = d_send[0]
@@ -305,19 +318,17 @@
             x = pieces(j).astype(F32)
             result[:, j * LANES : (j + 1) * LANES] = (x * inverse * gains[j : j + 1, :]).astype(BF16)
 
-    wait_bytes(c_recv.at[pl.ds(0, n_tp - 1)], c_sem.at[1])
-    normalise(lambda j: c_recv[j], n2, seqs)
-    ready(sg)
-    ready(su)
-    ready(sd)
-    hidden = (silu(dot_t(n2[...], sg[...])) * dot_t(n2[...], su[...])).astype(BF16)
-    down = dot(hidden, sd[...]).astype(BF16)
-    for q in range(n_tp):
-        s_send[q] = down[:, q * LANES : (q + 1) * LANES]
-    to_tp(lambda q: s_send.at[q], lambda k: s_recv.at[k - 1], s_sem)
-    ready(eg)
-    ready(eu)
-    ready(ed)
+    def shared():
+        wait_bytes(c_recv.at[pl.ds(0, n_tp - 1)], c_sem.at[1])
+        normalise(lambda j: c_recv[j], n2, seqs)
+        ready(sg)
+        ready(su)
+        ready(sd)
+        hidden = (silu(dot_t(n2[...], sg[...])) * dot_t(n2[...], su[...])).astype(BF16)
+        down = dot(hidden, sd[...]).astype(BF16)
+        for q in range(n_tp):
+            s_send[q] = down[:, q * LANES : (q + 1) * LANES]
+        to_tp(lambda q: s_send.at[q], lambda k: s_recv.at[k], s_sem)
 
     def gather(c):
         first = 1 if c == 0 else c * n_chunk
@@ -328,13 +339,15 @@
         e_recv[c, t] = block
 
     def experts(c):
+        if c == 0:
+            ready(eg, eu, ed)
         wait_bytes(e_recv.at[c, pl.ds(0, n_tp - 1)], e_sem.at[c, 1])
         normalise(lambda j: e_recv[c, j], xn, rows)
         hidden = (silu(dot_t(xn[...], eg[0])) * dot_t(xn[...], eu[0])).astype(BF16)
         down = dot(hidden, ed[0]).astype(BF16)
         for q in range(n_tp):
             g_send[c, q] = down[:, q * LANES : (q + 1) * LANES]
-        to_tp(lambda q: g_send.at[c, q], lambda k: g_recv.at[c, k - 1], g_sem.at[c])
+        to_tp(lambda q: g_send.at[c, q], lambda k: g_recv.at[c, k], g_sem.at[c])
 
     def give_back(c):
         wait_bytes(g_recv.at[c], g_sem.at[c, 1])
@@ -344,24 +357,27 @@
         h_send[c * n_chunk : (c + 1) * n_chunk] = total.reshape(n_chunk, 2, LANES).astype(BF16)
         first = 1 if c == 0 else c * n_chunk
 
-        def step(s, carry):
+        def step(s):
             i = (c + 1) * n_chunk - 1 - s
             back = lax.rem(p + n_ep - offset_of(i), n_ep)
             pltpu.make_async_remote_copy(
                 h_send.at[i], h_recv.at[i], h_sem.at[0], h_sem.at[1],
                 device_id=(back, t), device_id_type=MESH,
             ).start()
-            return carry
-
-        lax.fori_loop(0, (c + 1) * n_chunk - first, step, 0)
+
+        unrolled((c + 1) * n_chunk - first, step)
         if c == 0:
             h_recv[0] = h_send[0]
 
-    for c in range(chunks):
-        gather(c)
-        if c >= 1:
-            experts(c - 1)
-    experts(chunks - 1)
+    gather(0)
+    shared()
+    gather(1)
+    gather(2)
+    experts(0)
+    gather(3)
+    experts(1)
+    experts(2)
+    experts(3)
     for c in range(chunks):
         give_back(c)
 

time: 77.9 us -> 73.9 us (0.949)
  Pallas kernels: 75.5 us -> 71.6 us
    pallas_call x1, Pallas kernels: 75.5 us -> 71.6 us  [body(): pl.pallas_call(functools.partial(kernel, (n_ep, n_tp, heads, chunks)), ou...]
where the time goes in v3:
time: 73.9 us; the launch traced here: 73.8 us
  Pallas kernels  71.6 us (97%)
  local copies, waits for them, and re-layouts  1.56 us (2%)
    pallas_call x1, Pallas kernels, body(): pl.pallas_call(functools.partial(kernel, (n_ep, n_tp, heads, chunks)), ou...  71.6 us
    unnamed x2, local copies, waits for them, and re-layouts  1.56 us

profile of v3, /device:TPU:1, one launch (start us, length us, event | category | flops | bytes accessed | tf_op | source)
XLA Modules:
  0.0 73.8 jit_solution(11874018338412503012)
XLA Ops:
  0.6 71.6 %shard_map.212 = (bf16[16,128]{1,0:T(8,128)(2,1)S(1)}, bf16[16,256,128]{2,1,0:T(8,128)(2,1)S(1)}) custom-call(bf16[16,2048]{1,0:T(8,128)(2,1)} %tokens_h.1, bf16[16,256,128]{2,1,0:T(8,128)(2,1)} %state_h.1, bf16[16,128]{1,0:T(8,128)(2,1)} %bitcast.16, bf16[128,1024]{1,0:T(8,128)(2,1)} %wq_h.1, bf16[128,1024]{1,0:T(8,128)(2,1)} %wk_h.1, ...), custom_call_target="tpu_custom_call" | custom-call | tf_op jit(solution)/shard_map/pallas_call | solution.py:458
  72.2 0.6 copy.25
  72.8 1.0 %copy.26 = bf16[16,256,128]{2,1,0:T(8,128)(2,1)} copy(bf16[16,256,128]{2,1,0:T(8,128)(2,1)S(1)} %get-tuple-element.3) | data formatting | bytes 2097152

commit v4 on v3

--- a/solution.py
+++ b/solution.py
@@ -9,7 +9,8 @@
 
 EPSILON = 1e-06
 LANES = 128
-CHUNKS = 4
+GATHERED = (8, 8, 16, 16, 8, 8)
+TAKEN = (16, 16, 16, 8, 8)
 MESH = pl.DeviceIdType.MESH
 F32 = jnp.float32
 BF16 = jnp.bfloat16
@@ -33,19 +34,19 @@
     eg_h, eu_h, ed_h, sg_h, su_h, sd_h, ids_h, rw_h,
     out, newstate,
     tokens, state, gain1, wq, wk, wv, wo, wl, wd, bias, hgain, wout, gain2, eg, eu, ed, sg, su, sd, ids, rw,
-    normed, own_normed, a_send, a_recv, b_send, b_recv, c_send, c_recv, n2, s_send, s_recv,
-    d_send, d_recv, e_send, e_recv, xn, g_send, g_recv, h_send, h_recv,
-    in_sem, a_sem, b_sem, c_sem, s_sem, d_sem, e_sem, g_sem, h_sem, z_sem,
+    normed, own_normed, a_send, a_recv, q_send, q_recv, b_send, b_recv, c_send, c_recv, s_send, s_recv,
+    d_send, d_recv, e_send, e_recv, g_send, g_recv, h_send, h_recv,
+    in_sem, a_sem, q_sem, b_sem, c_sem, s_sem, d_sem, e_sem, g_sem, h_sem, z_sem,
 ):
-    n_ep, n_tp, heads, chunks = sizes
+    n_ep, n_tp, heads, counts, taken = sizes
+    starts = [sum(counts[:c]) for c in range(len(counts))]
+    taken_starts = [sum(taken[:c]) for c in range(len(taken))]
     seqs, width = tokens.shape
     dk, vc = state.shape[1], state.shape[2]
     blocks = width // LANES
     per_head = n_tp // heads
     head_width = vc * per_head
     slots = n_ep * 2
-    n_chunk = n_ep // chunks
-    rows = n_chunk * 2
     p = lax.axis_index("ep")
     t = lax.axis_index("tp")
     head = t // per_head
@@ -116,7 +117,7 @@
         pl.semaphore_signal(barrier, inc=1, device_id=(q, t), device_id_type=MESH)
     for q in tp_partners:
         pl.semaphore_signal(barrier, inc=1, device_id=(p, q), device_id_type=MESH)
-    for _, dst in pairs[2:12]:
+    for _, dst in pairs[2:4]:
         pltpu.make_async_copy(*loads[id(dst)]).start()
 
     rounds = []
@@ -144,9 +145,8 @@
         x = tokens[:, j * LANES : (j + 1) * LANES].astype(F32)
         normed[:, j * LANES : (j + 1) * LANES] = (x * inverse * gains[j : j + 1, :]).astype(BF16)
     own_normed[...] = normed[:, own_cols]
-
-    pl.semaphore_wait(barrier, n_tp - 1 + len(near))
-    tell(0)
+    for _, dst in pairs[4:12]:
+        pltpu.make_async_copy(*loads[id(dst)]).start()
 
     ready(wq)
     ready(wk)
@@ -156,6 +156,8 @@
         a_send[h, :, :dk] = query_part[:, h * dk : (h + 1) * dk]
         a_send[h, :, dk:] = key_part[:, h * dk : (h + 1) * dk]
 
+    pl.semaphore_wait(barrier, n_tp - 1 + len(near))
+    tell(0)
     to_tp(lambda q: a_send.at[q // per_head], lambda k: a_recv.at[k], a_sem)
 
     for _, dst in pairs[12:]:
@@ -236,17 +238,22 @@
         got = dot(both, state[b])
         read = read + jnp.where(row == b, got[:seqs] + got[seqs:], 0.0)
     read = read * dk**-0.5
-    own_squares = jnp.sum(read * read, axis=1, keepdims=True)
     mixed = (read * gate).astype(BF16)
     part = dot(mixed, wout[...]).astype(BF16)
-    sq_hi = own_squares.astype(BF16).astype(F32)
-    sq_lo = (own_squares - sq_hi).astype(BF16).astype(F32)
-    first_lanes = lax.broadcasted_iota(jnp.int32, (seqs, LANES), 1)
-    carried_squares = jnp.where(first_lanes == 0, sq_hi, jnp.where(first_lanes == 1, sq_lo, 0.0)).astype(BF16)
     for q in range(n_tp):
-        b_send[q, :seqs, :] = part[:, q * LANES : (q + 1) * LANES]
-        b_send[q, seqs:, :] = carried_squares
+        b_send[q] = part[:, q * LANES : (q + 1) * LANES]
     to_tp(lambda q: b_send.at[q], lambda k: b_recv.at[t], b_sem)
+    squared = read * read
+    squared_hi = squared.astype(BF16)
+    squared_lo = (squared - squared_hi.astype(F32)).astype(BF16)
+    ones = jnp.ones((2 * seqs, vc), BF16)
+    own_squares = dot_t(ones, jnp.concatenate([squared_hi, jnp.zeros((LANES - seqs, vc), BF16)], axis=0))
+    own_squares += dot_t(ones, jnp.concatenate([squared_lo, jnp.zeros((LANES - seqs, vc), BF16)], axis=0))
+    square_row = lax.broadcasted_iota(jnp.int32, own_squares.shape, 0)
+    square_hi = own_squares.astype(BF16).astype(F32)
+    q_send[...] = jnp.where(square_row == 0, square_hi, own_squares - square_hi)[:2].astype(BF16)
+    to_tp(lambda q: q_send, lambda k: q_recv.at[t], q_sem)
+    q_recv[t] = q_send[...]
     b_recv[t] = b_send[t]
 
     padded = jnp.concatenate(
@@ -278,17 +285,22 @@
 
     lax.fori_loop(0, seqs, update, 0)
 
+    wait_bytes(q_recv.at[pl.ds(0, n_tp - 1)], q_sem.at[1])
+    head_sums = []
+    for h in range(heads):
+        sums = jnp.zeros((2, LANES), F32)
+        for q in range(h * per_head, (h + 1) * per_head):
+            sums = sums + q_recv[q].astype(F32)
+        head_sums.append(jnp.sum(sums, axis=0, keepdims=True))
+    head_sums = jnp.concatenate(head_sums + [jnp.zeros((LANES - heads, LANES), F32)], axis=0).T[:seqs]
+    scales = lax.rsqrt(head_sums / head_width + EPSILON)
     wait_bytes(b_recv.at[pl.ds(0, n_tp - 1)], b_sem.at[1])
     second = tokens[:, own_cols].astype(F32)
     for h in range(heads):
         parts = jnp.zeros((seqs, LANES), F32)
-        sums = jnp.zeros((seqs, LANES), F32)
         for q in range(h * per_head, (h + 1) * per_head):
-            got = b_recv[q].astype(F32)
-            parts = parts + got[:seqs]
-            sums = sums + got[seqs:]
-        scale = lax.rsqrt(jnp.sum(sums, axis=1, keepdims=True) / head_width + EPSILON)
-        second = second + scale * parts
+            parts = parts + b_recv[q].astype(F32)
+        second = second + scales[:, h : h + 1] * parts
     second = second.astype(BF16)
     c_send[...] = second
 
@@ -296,90 +308,99 @@
 
     hear(3)
 
-    def dispatch(step):
-        i = n_ep - 1 - step
+    def dispatch(c, step):
+        i = starts[c] + counts[c] - 1 - step
         pltpu.make_async_remote_copy(
-            d_send.at[i], d_recv.at[i], d_sem.at[0], d_sem.at[1 + i // n_chunk],
+            d_send.at[i], d_recv.at[i], d_sem.at[0], d_sem.at[1 + c],
             device_id=(ep_peer(i), t), device_id_type=MESH,
         ).start()
 
-    unrolled(n_ep - 1, dispatch)
+    for c in range(len(counts) - 1, -1, -1):
+        unrolled(counts[c] - (c == 0), functools.partial(dispatch, c))
     to_tp(lambda q: c_send, lambda k: c_recv.at[t], c_sem)
     c_recv[t] = second
     d_recv[0] = d_send[0]
 
-    def normalise(pieces, result, count):
+    def scale_of(pieces, count):
         squares = jnp.zeros((count, LANES), F32)
-        for j in range(blocks):
-            x = pieces(j).astype(F32)
+        for piece in pieces:
+            x = piece.astype(F32)
             squares = squares + x * x
-        inverse = lax.rsqrt(jnp.sum(squares, axis=1, keepdims=True) / width + EPSILON)
-        for j in range(blocks):
-            x = pieces(j).astype(F32)
-            result[:, j * LANES : (j + 1) * LANES] = (x * inverse * gains[j : j + 1, :]).astype(BF16)
+        return lax.rsqrt(jnp.sum(squares, axis=1, keepdims=True) / width + EPSILON)
+
+    ready(eg, eu, sg, su)
+    for j in range(blocks):
+        cols = slice(j * LANES, (j + 1) * LANES)
+        for w in (eg.at[0], eu.at[0], sg, su):
+            w[:, cols] = (w[:, cols].astype(F32) * gains[j : j + 1, :]).astype(BF16)
+
+    def hidden_of(pieces, count, gate_w, up_w):
+        x = jnp.concatenate(pieces, axis=1)
+        scale = scale_of(pieces, count)
+        return (silu(dot_t(x, gate_w) * scale) * (dot_t(x, up_w) * scale)).astype(BF16)
 
     def shared():
         wait_bytes(c_recv.at[pl.ds(0, n_tp - 1)], c_sem.at[1])
-        normalise(lambda j: c_recv[j], n2, seqs)
-        ready(sg)
-        ready(su)
         ready(sd)
-        hidden = (silu(dot_t(n2[...], sg[...])) * dot_t(n2[...], su[...])).astype(BF16)
+        hidden = hidden_of([c_recv[j] for j in range(blocks)], seqs, sg[...], su[...])
         down = dot(hidden, sd[...]).astype(BF16)
         for q in range(n_tp):
             s_send[q] = down[:, q * LANES : (q + 1) * LANES]
         to_tp(lambda q: s_send.at[q], lambda k: s_recv.at[k], s_sem)
 
+    def sources(c):
+        return pl.ds(max(starts[c], 1), counts[c] - (c == 0))
+
     def gather(c):
-        first = 1 if c == 0 else c * n_chunk
-        wait_bytes(d_recv.at[pl.ds(first, (c + 1) * n_chunk - first)], d_sem.at[1 + c])
-        block = d_recv[c * n_chunk : (c + 1) * n_chunk].astype(F32).reshape(rows, LANES).astype(BF16)
-        e_send[c] = block
-        to_tp(lambda q: e_send.at[c], lambda k: e_recv.at[c, t], e_sem.at[c])
-        e_recv[c, t] = block
+        rows = pl.ds(2 * starts[c], 2 * counts[c])
+        wait_bytes(d_recv.at[sources(c)], d_sem.at[1 + c])
+        block = d_recv[starts[c] : starts[c] + counts[c]].astype(F32).reshape(2 * counts[c], LANES).astype(BF16)
+        e_send[rows] = block
+        to_tp(lambda q: e_send.at[rows], lambda k: e_recv.at[t, rows], e_sem.at[c])
+        e_recv[t, rows] = block
 
     def experts(c):
         if c == 0:
-            ready(eg, eu, ed)
-        wait_bytes(e_recv.at[c, pl.ds(0, n_tp - 1)], e_sem.at[c, 1])
-        normalise(lambda j: e_recv[c, j], xn, rows)
-        hidden = (silu(dot_t(xn[...], eg[0])) * dot_t(xn[...], eu[0])).astype(BF16)
+            ready(ed)
+        rows = pl.ds(2 * taken_starts[c], 2 * taken[c])
+        for m in range(len(counts)):
+            if taken_starts[c] <= starts[m] < taken_starts[c] + taken[c]:
+                some = pl.ds(2 * starts[m], 2 * counts[m])
+                wait_bytes(e_recv.at[pl.ds(0, n_tp - 1), some], e_sem.at[m, 1])
+        hidden = hidden_of([e_recv[j, rows] for j in range(blocks)], 2 * taken[c], eg[0], eu[0])
         down = dot(hidden, ed[0]).astype(BF16)
         for q in range(n_tp):
-            g_send[c, q] = down[:, q * LANES : (q + 1) * LANES]
-        to_tp(lambda q: g_send.at[c, q], lambda k: g_recv.at[c, k], g_sem.at[c])
+            g_send[q, rows] = down[:, q * LANES : (q + 1) * LANES]
+        to_tp(lambda q: g_send.at[q, rows], lambda k: g_recv.at[k, rows], g_sem.at[c])
 
     def give_back(c):
-        wait_bytes(g_recv.at[c], g_sem.at[c, 1])
-        total = g_send[c, t].astype(F32)
+        first, count = taken_starts[c], taken[c]
+        rows = pl.ds(2 * first, 2 * count)
+        wait_bytes(g_recv.at[pl.ds(0, n_tp - 1), rows], g_sem.at[c, 1])
+        total = g_send[t, rows].astype(F32)
         for k in range(n_tp - 1):
-            total = total + g_recv[c, k].astype(F32)
-        h_send[c * n_chunk : (c + 1) * n_chunk] = total.reshape(n_chunk, 2, LANES).astype(BF16)
-        first = 1 if c == 0 else c * n_chunk
+            total = total + g_recv[k, rows].astype(F32)
+        h_send[first : first + count] = total.reshape(count, 2, LANES).astype(BF16)
 
         def step(s):
-            i = (c + 1) * n_chunk - 1 - s
+            i = first + count - 1 - s
             back = lax.rem(p + n_ep - offset_of(i), n_ep)
             pltpu.make_async_remote_copy(
                 h_send.at[i], h_recv.at[i], h_sem.at[0], h_sem.at[1],
                 device_id=(back, t), device_id_type=MESH,
             ).start()
 
-        unrolled((c + 1) * n_chunk - first, step)
+        unrolled(count - (c == 0), step)
         if c == 0:
             h_recv[0] = h_send[0]
 
-    gather(0)
+    for c in range(len(counts)):
+        gather(c)
+    for c in range(len(taken)):
+        experts(c)
+    for c in range(len(taken)):
+        give_back(c)
     shared()
-    gather(1)
-    gather(2)
-    experts(0)
-    gather(3)
-    experts(1)
-    experts(2)
-    experts(3)
-    for c in range(chunks):
-        give_back(c)
 
     wait_bytes(s_recv, s_sem.at[1])
     total = s_send[t].astype(F32)
@@ -387,19 +408,29 @@
         total = total + s_recv[k].astype(F32)
     total = total + c_send[...].astype(F32)
     wait_bytes(a_recv, a_sem.at[0])
+    wait_bytes(q_recv.at[pl.ds(0, n_tp - 1)], q_sem.at[0])
     wait_bytes(b_recv.at[pl.ds(0, n_tp - 1)], b_sem.at[0])
     wait_bytes(c_recv.at[pl.ds(0, n_tp - 1)], c_sem.at[0])
     wait_bytes(s_recv, s_sem.at[0])
     wait_bytes(d_recv.at[pl.ds(1, n_ep - 1)], d_sem.at[0])
-    for c in range(chunks):
-        wait_bytes(e_recv.at[c, pl.ds(0, n_tp - 1)], e_sem.at[c, 0])
-        wait_bytes(g_recv.at[c], g_sem.at[c, 0])
+    for c in range(len(counts)):
+        wait_bytes(e_recv.at[pl.ds(0, n_tp - 1), pl.ds(2 * starts[c], 2 * counts[c])], e_sem.at[c, 0])
+    for c in range(len(taken)):
+        wait_bytes(g_recv.at[pl.ds(0, n_tp - 1), pl.ds(2 * taken_starts[c], 2 * taken[c])], g_sem.at[c, 0])
 
     wait_bytes(h_recv.at[pl.ds(1, n_ep - 1)], h_sem.at[1])
     returned = h_recv[...].astype(F32).reshape(slots, LANES).astype(BF16)
     total = total + dot(weight_hi, returned) + dot(weight_lo, returned)
     out[...] = total.astype(BF16)
     wait_bytes(h_recv.at[pl.ds(1, n_ep - 1)], h_sem.at[0])
+
+
+def finish(x, state_in, out, state_out, sem):
+    copies = [pltpu.make_async_copy(state_in, state_out, sem.at[0]), pltpu.make_async_copy(x, out, sem.at[1])]
+    for copy in copies:
+        copy.start()
+    for copy in copies:
+        copy.wait()
 
 
 def body(n_ep, n_tp, *args):
@@ -411,7 +442,8 @@
     seqs, width = tokens.shape
     dk = old_state.shape[1]
     heads = decay_weight.shape[1] // dk
-    chunks = CHUNKS
+    counts = tuple(n_ep * x // 64 for x in GATHERED)
+    taken = tuple(n_ep * x // 64 for x in TAKEN)
     blocks = width // LANES
     operands = [
         tokens, old_state, first_gain.reshape(blocks, LANES), query_weight, key_weight, value_weight, outgate_weight,
@@ -419,7 +451,7 @@
         second_gain.reshape(blocks, LANES), expert_gate.swapaxes(1, 2), expert_up.swapaxes(1, 2), expert_down,
         shared_gate.T, shared_up.T, shared_down, route_ids.T, route_weights.T,
     ]
-    rows = 2 * n_ep // chunks
+    rows = 2 * n_ep
     vmem = lambda shape, dtype=BF16: pltpu.VMEM(shape, dtype)
     dma = pltpu.SemaphoreType.DMA
     scratch = [vmem(x.shape, x.dtype) for x in operands]
@@ -428,20 +460,20 @@
         vmem((seqs, LANES)),
         vmem((heads, seqs, 2 * dk)),
         vmem((n_tp - 1, seqs, 2 * dk)),
-        vmem((n_tp, 2 * seqs, LANES)),
-        vmem((n_tp, 2 * seqs, LANES)),
+        vmem((2, LANES)),
+        vmem((n_tp, 2, LANES)),
+        vmem((n_tp, seqs, LANES)),
+        vmem((n_tp, seqs, LANES)),
         vmem((seqs, LANES)),
         vmem((n_tp, seqs, LANES)),
-        vmem((seqs, width)),
         vmem((n_tp, seqs, LANES)),
         vmem((n_tp - 1, seqs, LANES)),
         vmem((n_ep, 2, LANES)),
         vmem((n_ep, 2, LANES)),
-        vmem((chunks, rows, LANES)),
-        vmem((chunks, n_tp, rows, LANES)),
-        vmem((rows, width)),
-        vmem((chunks, n_tp, rows, LANES)),
-        vmem((chunks, n_tp - 1, rows, LANES)),
+        vmem((rows, LANES)),
+        vmem((n_tp, rows, LANES)),
+        vmem((n_tp, rows, LANES)),
+        vmem((n_tp - 1, rows, LANES)),
         vmem((n_ep, 2, LANES)),
         vmem((n_ep, 2, LANES)),
         dma((len(operands),)),
@@ -449,14 +481,15 @@
         dma((2,)),
         dma((2,)),
         dma((2,)),
-        dma((1 + chunks,)),
-        dma((chunks, 2)),
-        dma((chunks, 2)),
+        dma((2,)),
+        dma((1 + len(counts),)),
+        dma((len(counts), 2)),
+        dma((len(taken), 2)),
         dma((2,)),
         pltpu.SemaphoreType.REGULAR((4,)),
     ]
-    return pl.pallas_call(
-        functools.partial(kernel, (n_ep, n_tp, heads, chunks)),
+    results = pl.pallas_call(
+        functools.partial(kernel, (n_ep, n_tp, heads, counts, taken)),
         out_shape=(
             pltpu.VMEM((seqs, LANES), BF16),
             pltpu.VMEM(old_state.shape, BF16),
@@ -468,6 +501,17 @@
             collective_id=0, has_side_effects=True
         ),
     )(*operands)
+    results = [pltpu.with_memory_space_constraint(x, pltpu.VMEM) for x in results]
+    return pl.pallas_call(
+        finish,
+        out_shape=(
+            jax.ShapeDtypeStruct((seqs, LANES), BF16),
+            jax.ShapeDtypeStruct(old_state.shape, BF16),
+        ),
+        in_specs=[pl.BlockSpec(memory_space=pl.ANY), pl.BlockSpec(memory_space=pl.ANY)],
+        out_specs=(pl.BlockSpec(memory_space=pltpu.HBM), pl.BlockSpec(memory_space=pltpu.HBM)),
+        scratch_shapes=[dma((2,))],
+    )(*results)
 
 
 def solution(mesh):

time: 73.9 us -> 72 us (0.974)
  local copies, waits for them, and re-layouts: 1.56 us -> 0 us
    unnamed x2 -> x0, local copies, waits for them, and re-layouts: 1.56 us -> none
    pallas_call x1 -> x2, Pallas kernels: 71.6 us -> 71.2 us  [the longest x1 70.2 us: body(): pl.pallas_call(functools.partial(kernel, (n_ep, n_tp, heads, counts, take...]
where the time goes in v4:
time: 72 us; the launch traced here: 71.8 us
  Pallas kernels  71.2 us (99%)
    pallas_call x1, Pallas kernels, body(): pl.pallas_call(functools.partial(kernel, (n_ep, n_tp, heads, counts, take...  70.2 us

profile of v4, /device:TPU:1, one launch (start us, length us, event | category | flops | bytes accessed | tf_op | source)
XLA Modules:
  0.0 71.8 jit_solution(12642557345172459543)
XLA Ops:
  0.6 70.2 %shard_map.212 = (bf16[16,128]{1,0:T(8,128)(2,1)S(1)}, bf16[16,256,128]{2,1,0:T(8,128)(2,1)S(1)}) custom-call(bf16[16,2048]{1,0:T(8,128)(2,1)} %tokens_h.1, bf16[16,256,128]{2,1,0:T(8,128)(2,1)} %state_h.1, bf16[16,128]{1,0:T(8,128)(2,1)} %bitcast.16, bf16[128,1024]{1,0:T(8,128)(2,1)} %wq_h.1, bf16[128,1024]{1,0:T(8,128)(2,1)} %wk_h.1, ...), custom_call_target="tpu_custom_call" | custom-call | tf_op jit(solution)/shard_map/pallas_call | solution.py:491
  70.8 1.0 %shard_map.213 = (bf16[16,128]{1,0:T(8,128)(2,1)}, bf16[16,256,128]{2,1,0:T(8,128)(2,1)}) custom-call(bf16[16,128]{1,0:T(8,128)(2,1)S(1)} %get-tuple-element.4.x, bf16[16,256,128]{2,1,0:T(8,128)(2,1)S(1)} %get-tuple-element.5.state_in), custom_call_target="tpu_custom_call" | custom-call | tf_op jit(solution)/shard_map/pallas_call | solution.py:505

commit v5 on v4

--- a/solution.py
+++ b/solution.py
@@ -398,9 +398,9 @@
         gather(c)
     for c in range(len(taken)):
         experts(c)
+    shared()
     for c in range(len(taken)):
         give_back(c)
-    shared()
 
     wait_bytes(s_recv, s_sem.at[1])
     total = s_send[t].astype(F32)

time: 72 us -> 72 us (level)
  no operation moved by 1% of the time
where the time goes in v5:
time: 72 us; the launch traced here: 71.8 us
  Pallas kernels  71.2 us (99%)
    pallas_call x1, Pallas kernels, body(): pl.pallas_call(functools.partial(kernel, (n_ep, n_tp, heads, counts, take...  70.2 us

profile of v5, /device:TPU:1, one launch (start us, length us, event | category | flops | bytes accessed | tf_op | source)
XLA Modules:
  0.0 71.8 jit_solution(2087547463507990292)
XLA Ops:
  0.6 70.2 %shard_map.212 = (bf16[16,128]{1,0:T(8,128)(2,1)S(1)}, bf16[16,256,128]{2,1,0:T(8,128)(2,1)S(1)}) custom-call(bf16[16,2048]{1,0:T(8,128)(2,1)} %tokens_h.1, bf16[16,256,128]{2,1,0:T(8,128)(2,1)} %state_h.1, bf16[16,128]{1,0:T(8,128)(2,1)} %bitcast.16, bf16[128,1024]{1,0:T(8,128)(2,1)} %wq_h.1, bf16[128,1024]{1,0:T(8,128)(2,1)} %wk_h.1, ...), custom_call_target="tpu_custom_call" | custom-call | tf_op jit(solution)/shard_map/pallas_call | solution.py:491
  70.8 1.0 %shard_map.213 = (bf16[16,128]{1,0:T(8,128)(2,1)}, bf16[16,256,128]{2,1,0:T(8,128)(2,1)}) custom-call(bf16[16,128]{1,0:T(8,128)(2,1)S(1)} %get-tuple-element.4.x, bf16[16,256,128]{2,1,0:T(8,128)(2,1)S(1)} %get-tuple-element.5.state_in), custom_call_target="tpu_custom_call" | custom-call | tf_op jit(solution)/shard_map/pallas_call | solution.py:505
